TPU v7x, 32 devices: a whole 2x2x4 slice. The times are simulated.
32 devices in a mesh: ep: 8 (over z, x), tp: 4 (over y, core).
Axes of the slice: x: 2, y: 2, z: 4, core: 2. Of those that a mesh axis runs over, the one named last changes fastest.
Arguments:
- mix_in: bfloat16 [4096, 2048], P('ep'), may hold values from -6 to 6
- forget_shift: float32 [4096], P('ep'), may hold values from -2.5 to 2.5, as said below
- mix_gain: float32 [2048], replicated, may hold values from 0.1 to 1.9
- w_query: bfloat16 [2048, 1024], P(None, 'tp'), may hold values from -0.125 to 0.125
- w_forget: bfloat16 [2048, 1024], P(None, 'tp'), may hold values from -0.125 to 0.125
- w_value: bfloat16 [2048, 1024], P(None, 'tp'), may hold values from -0.125 to 0.125
- forget_room: float32 [1024], P('tp'), may hold values from 0 to 1, as said below
- head_gain: float32 [1024], P('tp'), may hold values from 0.1 to 1.9
- w_out: bfloat16 [1024, 2048], P('tp'), may hold values from -0.1875 to 0.1875
- moe_in: bfloat16 [2048, 2048], P('ep'), may hold values from -6 to 6
- moe_gain: float32 [2048], replicated, may hold values from 0.1 to 1.9
- expert_choice: int32 [2048, 4], P('ep'), may hold values from 0 to 7, as said below
- route_logit: float32 [2048, 4], P(('ep', 'tp')), may hold values from -6 to 6
- w_exp_gate: bfloat16 [8, 2048, 1024], P('ep', None, 'tp'), may hold values from -0.125 to 0.125
- w_exp_up: bfloat16 [8, 2048, 1024], P('ep', None, 'tp'), may hold values from -0.125 to 0.125
- w_exp_down: bfloat16 [8, 1024, 2048], P('ep', 'tp'), may hold values from -0.1875 to 0.1875
- w_sh_gate: bfloat16 [2048, 512], P(None, 'tp'), may hold values from -0.125 to 0.125
- w_sh_up: bfloat16 [2048, 512], P(None, 'tp'), may hold values from -0.125 to 0.125
- w_sh_down: bfloat16 [512, 2048], P('tp'), may hold values from -0.25 to 0.25
Outputs:
- mixer_out: bfloat16 [4096, 2048], P(('ep', 'tp'))
- moe_out: bfloat16 [2048, 2048], P(('ep', 'tp'))
Inputs may be any that keep to these rules, and one draw needn't show every extreme that they name: `forget_room`: positive and at most 1/6 in every entry. `forget_shift`: constant over each aligned span of 64 positions. `expert_choice`: each row names 4 different experts. In each aligned block of 64 rows no expert is named by more than 48 rows; in every draw one expert is named by exactly 48 rows in every block.
All inputs are finite; a program needn't handle non-finite values.
Results may differ from a plain program's by a relative error of at most 0.02.
Values may be sent and summed in bfloat16 or wider, within the bound.
A program may use at most 128 MiB of HBM per device.

v0:
```python
import functools

import jax
import jax.numpy as jnp
from jax import lax
from jax.experimental import pallas as pl
from jax.experimental.pallas import tpu as pltpu
from jax.sharding import PartitionSpec as P


HEAD = 64
SPAN = 64

epsilon = 1e-06
route_scale = 2.5


NT = (((1,), (1,)), ((), ()))
TN = (((0,), (0,)), ((), ()))
NN = (((1,), (0,)), ((), ()))


def dot(a, b, dims=NN):
    return lax.dot_general(
        a.astype(jnp.bfloat16),
        b.astype(jnp.bfloat16),
        dims,
        preferred_element_type=jnp.float32,
    )


def two_part(x):
    high = x.astype(jnp.bfloat16)
    return high, (x - high.astype(jnp.float32)).astype(jnp.bfloat16)


def head_mask(rows, columns):
    row = lax.broadcasted_iota(jnp.int32, (rows, columns), 0) // HEAD
    column = lax.broadcasted_iota(jnp.int32, (rows, columns), 1) // HEAD
    return row == column


def norm_rows(row_data, gain_vec):
    widened = row_data.astype(jnp.float32)
    scaled = widened * lax.rsqrt(jnp.mean(widened * widened, axis=-1, keepdims=True) + epsilon)
    return (scaled * gain_vec).astype(jnp.bfloat16)


def local_scan(
    x_ref, shift_ref, gain_ref, wq_ref, wf_ref, wv_ref, room_ref,
    mixed_ref, query_ref, carry_ref, state, decay,
):
    step = pl.program_id(0)
    width = wq_ref.shape[1]
    heads = width // HEAD

    @pl.when(step == 0)
    def _():
        state[...] = jnp.zeros_like(state)
        decay[...] = jnp.ones_like(decay)

    normed = norm_rows(x_ref[...], gain_ref[...])
    queries = dot(normed, wq_ref[...])
    queries = queries / (1.0 + jnp.exp(-queries))
    before = dot(normed, wf_ref[...]) + shift_ref[...]
    values = dot(normed, wv_ref[...])
    rate = room_ref[...] / (1.0 + jnp.exp(before))
    log_forget = jnp.log1p(-rate)
    causal = (
        lax.broadcasted_iota(jnp.int32, (SPAN, SPAN), 0)
        >= lax.broadcasted_iota(jnp.int32, (SPAN, SPAN), 1)
    )
    lower = causal.astype(jnp.bfloat16)
    high, low = two_part(log_forget)
    log_decay = dot(lower, high) + dot(lower, low)
    middle = log_decay[SPAN // 2 : SPAN // 2 + 1]
    block_end = log_decay[SPAN - 1 :]
    left = (queries * jnp.exp(log_decay - middle)).astype(jnp.bfloat16)
    right = rate * jnp.exp(middle - log_decay)
    mask = head_mask(width, width)
    stacked = jnp.concatenate([left] * heads, axis=0)
    stacked = jnp.where(mask, stacked, jnp.zeros_like(stacked))
    scores = dot(stacked, right, NT)
    scores = jnp.where(jnp.concatenate([causal] * heads, axis=0), scores, 0.0)
    spread = jnp.where(mask, dot(scores, values), 0.0)
    within = spread[:SPAN]
    for head in range(1, heads):
        within = within + spread[head * SPAN : (head + 1) * SPAN]
    query_decay = queries * jnp.exp(log_decay)
    mixed_ref[...] = within + dot(query_decay, state[...], NT)
    query_ref[...] = (query_decay * decay[...]).astype(jnp.bfloat16)
    added = dot(values, rate * jnp.exp(block_end - log_decay), TN)
    total = jnp.exp(block_end)
    new_state = total * state[...] + jnp.where(mask, added, 0.0)
    state[...] = new_state
    decay[...] = decay[...] * total

    @pl.when(step == pl.num_programs(0) - 1)
    def _():
        packed = new_state[:HEAD]
        for head in range(1, heads):
            packed = packed + new_state[head * HEAD : (head + 1) * HEAD]
        high, low = two_part(decay[...])
        row = lax.broadcasted_iota(jnp.int32, (16, width), 0)
        tail = jnp.where(row == 0, high.astype(jnp.float32), 0.0)
        tail = jnp.where(row == 1, low.astype(jnp.float32), tail)
        carry_ref[:HEAD] = packed.astype(jnp.bfloat16)
        carry_ref[HEAD:] = tail.astype(jnp.bfloat16)


def finish(mixed_ref, query_ref, all_ref, gain_ref, out_w_ref, part_ref, start):
    width = mixed_ref.shape[1]
    heads = width // HEAD
    mask = head_mask(width, width)

    @pl.when(pl.program_id(0) == 0)
    def _():
        def one(lap, state):
            block = all_ref[lap].astype(jnp.float32)
            total = block[HEAD : HEAD + 1] + block[HEAD + 1 : HEAD + 2]
            return total * state + block[:HEAD]

        packed = lax.fori_loop(
            0, all_ref.shape[0], one, jnp.zeros((HEAD, width), jnp.float32)
        )
        whole = jnp.concatenate([packed] * heads, axis=0)
        start[...] = jnp.where(mask, whole, 0.0).astype(jnp.bfloat16)

    mixed = mixed_ref[...] + dot(query_ref[...], start[...], NT)
    ones = mask.astype(jnp.bfloat16)
    high, low = two_part(mixed * mixed)
    square = (dot(high, ones) + dot(low, ones)) * (1.0 / HEAD)
    head_out = (mixed * lax.rsqrt(square + epsilon) * gain_ref[...]).astype(jnp.bfloat16)
    part_ref[...] = dot(head_out, out_w_ref[...]).astype(jnp.bfloat16)


def whole_block(array):
    return pl.BlockSpec(array.shape, lambda i, rank=array.ndim: (0,) * rank)


def mixer_scan(mix_in, forget_shift, mix_gain, w_query, w_forget, w_value, forget_room):
    rows, width = mix_in.shape[0], w_query.shape[1]
    gain = mix_gain[None]
    room = forget_room[None]
    by_span = lambda columns: pl.BlockSpec((SPAN, columns), lambda i: (i, 0))
    return pl.pallas_call(
        local_scan,
        grid=(rows // SPAN,),
        in_specs=[
            by_span(mix_in.shape[1]), by_span(1), whole_block(gain), whole_block(w_query),
            whole_block(w_forget), whole_block(w_value), whole_block(room),
        ],
        out_specs=[
            by_span(width), by_span(width),
            pl.BlockSpec((HEAD + 16, width), lambda i: (0, 0)),
        ],
        out_shape=[
            jax.ShapeDtypeStruct((rows, width), jnp.float32),
            jax.ShapeDtypeStruct((rows, width), jnp.bfloat16),
            jax.ShapeDtypeStruct((HEAD + 16, width), jnp.bfloat16),
        ],
        scratch_shapes=[
            pltpu.VMEM((width, width), jnp.float32),
            pltpu.VMEM((1, width), jnp.float32),
        ],
        compiler_params=pltpu.CompilerParams(vmem_limit_bytes=32 * 1024 * 1024),
        cost_estimate=pl.CostEstimate(
            flops=40_000_000_000 * rows // 512, bytes_accessed=7_000_000, transcendentals=0
        ),
        name="mixer_scan",
    )(mix_in, forget_shift[:, None], gain, w_query, w_forget, w_value, room)


def mixer_finish(mixed, query, carried, head_gain, w_out):
    rows, width = mixed.shape
    block = min(rows, 4 * SPAN)
    gain = head_gain[None]
    by_rows = lambda columns: pl.BlockSpec((block, columns), lambda i: (i, 0))
    return pl.pallas_call(
        finish,
        grid=(rows // block,),
        in_specs=[
            by_rows(width), by_rows(width),
            whole_block(carried), whole_block(gain), whole_block(w_out),
        ],
        out_specs=by_rows(w_out.shape[1]),
        out_shape=jax.ShapeDtypeStruct((rows, w_out.shape[1]), jnp.bfloat16),
        scratch_shapes=[pltpu.VMEM((width, width), jnp.bfloat16)],
        compiler_params=pltpu.CompilerParams(vmem_limit_bytes=32 * 1024 * 1024),
        cost_estimate=pl.CostEstimate(
            flops=4_000_000_000, bytes_accessed=5_000_000, transcendentals=0
        ),
        name="mixer_finish",
    )(mixed, query, carried, gain, w_out)


def swap(x, axis, bit):
    return lax.ppermute(x, axis, [(i, i ^ bit) for i in range(lax.axis_size(axis))])


def axis_bits(axis):
    return [1 << i for i in range(lax.axis_size(axis).bit_length() - 1)]


def split_bits(part, axis):
    bits = axis_bits(axis)
    rows = part.shape[0] >> len(bits)
    return part.reshape((2,) * len(bits) + (rows, part.shape[1])), bits[::-1]


def halve(held, axis, bit):
    part, bits = held
    part = part.astype(jnp.bfloat16)
    at = bits.index(bit)
    mine = (lax.axis_index(axis) // bit) % 2
    keep = lax.dynamic_index_in_dim(part, mine, at, False)
    send = lax.dynamic_index_in_dim(part, 1 - mine, at, False)
    total = keep.astype(jnp.float32) + swap(send, axis, bit).astype(jnp.float32)
    return total, [b for b in bits if b != bit]


def halve_all(held, axis, order):
    for bit in order:
        held = halve(held, axis, bit)
    return held[0]


def gather_rows(x, axis, order):
    bits = []
    for bit in order:
        at = sum(b > bit for b in bits)
        x = jnp.stack([x, swap(x, axis, bit)], axis=at)
        bits = sorted(bits + [bit], reverse=True)
    return x.reshape(-1, x.shape[-1])


def scatter_rows(part, axis, order):
    bits = axis_bits(axis)[::-1]
    part = part.reshape((2,) * len(bits) + (part.shape[0] >> len(bits), part.shape[1]))
    for bit in order:
        at = bits.index(bit)
        part = part.astype(jnp.bfloat16)
        keep = lax.index_in_dim(part, 0, at, False).astype(jnp.float32)
        part = keep + swap(lax.index_in_dim(part, 1, at, False), axis, bit).astype(jnp.float32)
        bits = [b for b in bits if b != bit]
    return part


def gather_groups(w):
    bits = axis_bits("tp")
    near, far = bits[0], bits[1:]
    away = []
    for bit in far[::-1]:
        away = away + [swap(x, "tp", bit) for x in [w] + away]
    home = [w, swap(w, "tp", near)]
    return home, [y for x in away for y in (x, swap(x, "tp", near))]


def carried_blocks(carry):
    count = lax.axis_size("ep")
    if count > 8:
        held = lax.all_gather(carry, "ep")
        before = jnp.arange(count)[:, None, None] < lax.axis_index("ep")
        return jnp.where(before, held, jnp.zeros_like(held))
    return jnp.stack(
        [
            lax.ppermute(carry, "ep", [(i, i + d) for i in range(count - d)])
            for d in range(count - 1, 0, -1)
        ]
    )


def hidden_units(left_ref, right_ref, *refs):
    count = (len(refs) - 1) // 2
    act_ref = refs[-1]
    rows = jnp.concatenate([left_ref[...], right_ref[...]], axis=1)
    width = refs[0].shape[1]
    for group in range(count):
        gate = dot(rows, refs[group][...])
        up = dot(rows, refs[count + group][...])
        act = gate / (1.0 + jnp.exp(-gate)) * up
        act_ref[:, group * width : (group + 1) * width] = act.astype(jnp.bfloat16)


def expert_units(left, right, gates, ups):
    rows, model, width = left.shape[0], gates[0].shape[0], gates[0].shape[1]
    block = min(rows, 256)
    count = len(gates)
    return pl.pallas_call(
        hidden_units,
        grid=(rows // block,),
        in_specs=[pl.BlockSpec((block, model // 2), lambda i: (i, 0))] * 2
        + [whole_block(w) for w in gates + ups],
        out_specs=pl.BlockSpec((block, count * width), lambda i: (i, 0)),
        out_shape=jax.ShapeDtypeStruct((rows, count * width), jnp.bfloat16),
        compiler_params=pltpu.CompilerParams(vmem_limit_bytes=40 * 1024 * 1024),
        cost_estimate=pl.CostEstimate(
            flops=4 * rows * model * width * count,
            bytes_accessed=2 * (2 * count * model * width + rows * model),
            transcendentals=0,
        ),
        name="expert_units",
    )(left, right, *gates, *ups)


def weighted_rows(experts, place_ref, share_ref, *refs):
    out_ref = refs[-1]
    acts = jnp.concatenate([ref[...] for ref in refs[:2]], axis=1)
    downs = refs[2:-1]
    width = downs[0].shape[0]
    result = dot(acts[:, :width], downs[0][...])
    for group in range(1, len(downs)):
        result = result + dot(acts[:, group * width : (group + 1) * width], downs[group][...])
    lane = lax.broadcasted_iota(jnp.int32, share_ref.shape, 1)
    chosen = (lane == place_ref[0]) | (lane == place_ref[0] + experts)
    share = jnp.sum(
        jnp.where(chosen, share_ref[...].astype(jnp.float32), 0.0), axis=1, keepdims=True
    )
    out_ref[...] = (result * share).astype(jnp.bfloat16)


def expert_rows(place, gathered, model, experts, acts, downs):
    rows, columns = gathered.shape[0], downs[0].shape[1]
    spare = gathered.shape[1] - model
    block = min(rows, 256)
    return pl.pallas_call(
        functools.partial(weighted_rows, experts),
        grid=(rows // block,),
        in_specs=[
            pl.BlockSpec(memory_space=pltpu.SMEM),
            pl.BlockSpec((block, spare), lambda i: (i, model // spare)),
        ]
        + [pl.BlockSpec((block, act.shape[1]), lambda i: (i, 0)) for act in acts]
        + [whole_block(w) for w in downs],
        out_specs=pl.BlockSpec((block, columns), lambda i: (i, 0)),
        out_shape=jax.ShapeDtypeStruct((rows, columns), jnp.bfloat16),
        compiler_params=pltpu.CompilerParams(vmem_limit_bytes=40 * 1024 * 1024),
        cost_estimate=pl.CostEstimate(
            flops=2 * rows * columns * (acts[0].shape[1] + acts[1].shape[1]),
            bytes_accessed=8_000_000,
            transcendentals=0,
        ),
        name="expert_rows",
    )(place, gathered, *acts, *downs)


def local(
    mix_in, forget_shift, mix_gain, w_query, w_forget, w_value, forget_room, head_gain, w_out,
    moe_in, moe_gain, expert_choice, route_logit, w_exp_gate, w_exp_up, w_exp_down,
    w_sh_gate, w_sh_up, w_sh_down,
):
    tp_count = lax.axis_size("tp")
    rank = lax.axis_index("tp")
    place = lax.axis_index("ep")
    experts = lax.axis_size("ep") * w_exp_gate.shape[0]
    quarter = moe_in.shape[0] // tp_count
    model = moe_in.shape[1]

    half = model // 2
    flat = lambda w: w.reshape(w.shape[1:])
    gates, far_gates = gather_groups(flat(w_exp_gate))
    ups, far_ups = gather_groups(flat(w_exp_up))
    left_downs = sum(gather_groups(flat(w_exp_down)[:, :half]), [])
    right_downs = sum(gather_groups(flat(w_exp_down)[:, half:]), [])

    hidden = norm_rows(moe_in, moe_gain)
    chance = jax.nn.sigmoid(route_logit)
    weights = chance / jnp.sum(chance, axis=-1, keepdims=True) * route_scale
    own_choice = lax.dynamic_slice_in_dim(expert_choice, rank * quarter, quarter, 0)
    table = jnp.sum(
        jnp.where(
            own_choice[..., None] == jnp.arange(experts, dtype=jnp.int32),
            weights[..., None],
            0.0,
        ),
        axis=1,
    )
    high, low = two_part(table)
    spare = -(2 * experts) % 128
    own_rows = lax.dynamic_slice_in_dim(hidden, rank * quarter, quarter, 0)
    sent = jnp.concatenate(
        [own_rows[:, half:], high, low, jnp.zeros((quarter, spare), jnp.bfloat16)], axis=1
    )
    ep_bits = axis_bits("ep")
    turned = ep_bits[1:] + ep_bits[:1]
    left_rows = gather_rows(own_rows[:, :half], "ep", ep_bits)
    right_rows = gather_rows(sent, "ep", turned)

    mixed, query, carry = mixer_scan(
        mix_in, forget_shift, mix_gain, w_query, w_forget, w_value, forget_room
    )
    mixer_part = mixer_finish(mixed, query, carried_blocks(carry), head_gain, w_out)
    shared_gate = jnp.dot(hidden, w_sh_gate, preferred_element_type=jnp.float32)
    shared_up = jnp.dot(hidden, w_sh_up, preferred_element_type=jnp.float32)
    shared_act = (jax.nn.silu(shared_gate) * shared_up).astype(jnp.bfloat16)
    shared_part = jnp.dot(shared_act, w_sh_down, preferred_element_type=jnp.float32)
    tp_bits = axis_bits("tp")
    mixer_held, mixer_bits = halve(split_bits(mixer_part, "tp"), "tp", tp_bits[0])
    shared_held, shared_bits = halve(split_bits(shared_part, "tp"), "tp", tp_bits[0])
    mixer_held, shared_held = mixer_held.astype(jnp.bfloat16), shared_held.astype(jnp.bfloat16)

    left_rows, right_rows, mixer_held, shared_held = lax.optimization_barrier(
        (left_rows, right_rows, mixer_held, shared_held)
    )
    home_act = expert_units(left_rows, right_rows, gates, ups)
    away_act = expert_units(left_rows, right_rows, far_gates, far_ups)
    acts = [home_act, away_act]
    spot = place[None].astype(jnp.int32)
    left = expert_rows(spot, right_rows, half, experts, acts, left_downs)
    right = expert_rows(spot, right_rows, half, experts, acts, right_downs)

    right, mixer_held, shared_held = lax.optimization_barrier((right, mixer_held, shared_held))
    left = scatter_rows(left, "ep", ep_bits)
    right = scatter_rows(right, "ep", turned)
    mixer_sum = halve_all((mixer_held, mixer_bits), "tp", tp_bits[1:])
    shared_sum = halve_all((shared_held, shared_bits), "tp", tp_bits[1:])
    routed = jnp.concatenate([left, right], axis=1)
    return (mixer_sum.astype(jnp.bfloat16), (routed + shared_sum).astype(jnp.bfloat16))


def solution(mesh):
    return jax.shard_map(
        local,
        mesh=mesh,
        in_specs=(
            P("ep", None),
            P("ep"),
            P(),
            P(None, "tp"),
            P(None, "tp"),
            P(None, "tp"),
            P("tp"),
            P("tp"),
            P("tp", None),
            P("ep", None),
            P(),
            P("ep", None),
            P(("ep", "tp"), None),
            P("ep", None, "tp"),
            P("ep", None, "tp"),
            P("ep", "tp", None),
            P(None, "tp"),
            P(None, "tp"),
            P("tp", None),
        ),
        out_specs=(P(("ep", "tp"), None), P(("ep", "tp"), None)),
        check_vma=False,
    )
```

profile of v0, /device:TPU:0, one launch (start us, length us, event | category | flops | bytes accessed | tf_op | source)
XLA Modules:
  0.0 178.9 jit_solution(10200320182855409288)
XLA Ops:
  0.6 0.9 copy.43.shift_ref
  1.5 1.6 copy-done.1
  3.1 1.2 copy-done.2
  4.4 1.2 copy-done.3
  5.6 1.2 copy-done.4
  6.8 0.7 copy-done.6
  7.5 0.7 copy-done.7
  8.2 9.8 %mixer_scan.1 = (f32[512,256]{1,0:T(8,128)S(1)}, bf16[512,256]{1,0:T(8,128)(2,1)S(1)}, bf16[80,256]{1,0:T(8,128)(2,1)S(1)}) custom-call(bf16[512,2048]{1,0:T(8,128)(2,1)S(1)} %copy-done.1, f32[512,1]{1,0:T(8,128)S(1)} %copy.43.shift_ref, f32[1,2048]{1,0:T(1,128)S(1)} %bitcast.131, bf16[2048,256]{1,0:T(8,128)(2,1)S(1)} %copy-done.2, ...), custom_call_target="tpu_custom_call" | custom-call | flops 40000000000 | bytes 7000000 | tf_op jit(solution)/shard_map/mixer_scan/pallas_call | solution.py:146
  18.0 0.8 copy-done.9
  18.8 8.6 %collective-permute-start.6 = (bf16[80,256]{1,0:T(8,128)(2,1)S(1)}, bf16[80,256]{1,0:T(8,128)(2,1)}, u32[]{:S(2)}, u32[]{:S(2)}) collective-permute-start(bf16[80,256]{1,0:T(8,128)(2,1)S(1)} %get-tuple-element.14), channel_id=1, source_target_pairs={{0,28},{1,29},{2,30},{3,31}} | collective-permute-start | bytes 122888 | tf_op jit(solution)/shard_map/ppermute | solution.py:267
  27.5 1.9 %collective-permute-start.7 = (bf16[80,256]{1,0:T(8,128)(2,1)S(1)}, bf16[80,256]{1,0:T(8,128)(2,1)}, u32[]{:S(2)}, u32[]{:S(2)}) collective-permute-start(bf16[80,256]{1,0:T(8,128)(2,1)S(1)} %get-tuple-element.14), channel_id=1, source_target_pairs={{0,24},{4,28},{1,25},{5,29},{2,26},{6,30},{3,27},{7,31}} | collective-permute-start | bytes 122888 | tf_op jit(solution)/shard_map/ppermute | solution.py:267
  29.3 1.9 %collective-permute-start.8 = (bf16[80,256]{1,0:T(8,128)(2,1)S(1)}, bf16[80,256]{1,0:T(8,128)(2,1)}, u32[]{:S(2)}, u32[]{:S(2)}) collective-permute-start(bf16[80,256]{1,0:T(8,128)(2,1)S(1)} %get-tuple-element.14), channel_id=1, source_target_pairs={{0,20},{4,24},{8,28},{1,21},{5,25},{9,29},{2,22},{6,26},{10,30},{3... | collective-permute-start | bytes 122888 | tf_op jit(solution)/shard_map/ppermute | solution.py:267
  31.3 1.3 collective-permute-start.9
  32.6 1.3 collective-permute-start.10
  34.3 0.9 fusion.24
  35.5 2.1 %fusion.26 = f32[256,128]{1,0:T(8,128)} fusion(bf16[256,2048]{1,0:T(8,128)(2,1)S(1)} %fusion.2, bf16[2048,128]{1,0:T(8,128)(2,1)} %param.35), kind=kOutput, calls=%fused_computation.79 | convolution fusion | flops 134217728 | bytes 1703936 | tf_op jit(solution)/shard_map/dot_general | solution.py:393
  37.7 1.8 %convolution_convert_fusion = bf16[256,2048]{1,0:T(8,128)(2,1)S(1)} fusion(bf16[128,2048]{1,0:T(8,128)(2,1)S(1)} %copy-done, bf16[256,2048]{1,0:T(8,128)(2,1)S(1)} %fusion.2, bf16[2048,128]{1,0:T(8,128)(2,1)} %param.36, f32[256,128]{1,0:T(8,128)} %fusion.26), kind=kOutput, calls=%fused_computation.2 | convolution fusion | flops 269156352 | bytes 3276800 | tf_op jit(solution)/shard_map/dot_general | solution.py:396
  39.5 1.0 dynamic-slice_bitcast_fusion.2
  40.5 0.7 fusion.25
  41.4 1.0 concatenate.6
  42.5 1.3 collective-permute-start.11
  43.8 0.8 bitcast_dynamic-update-slice_fusion.6
  44.5 2.5 %collective-permute-start.12 = (bf16[80,256]{1,0:T(8,128)(2,1)S(1)}, bf16[80,256]{1,0:T(8,128)(2,1)S(1)}, u32[]{:S(2)}, u32[]{:S(2)}) collective-permute-start(bf16[80,256]{1,0:T(8,128)(2,1)S(1)} %get-tuple-element.14), channel_id=1, source_target_pairs={{0,4},{4,8},{8,12},{12,16},{16,20},{20,24},{24,28},{1,5},{5,9},{9,... | collective-permute-start | bytes 122888 | tf_op jit(solution)/shard_map/ppermute | solution.py:267
  47.0 0.8 bitcast_dynamic-update-slice_fusion.5
  47.8 0.8 bitcast_dynamic-update-slice_fusion.4
  48.6 1.0 collective-permute-start
  49.6 1.5 collective-permute-start.17
  51.1 3.6 %collective-permute-done = bf16[64,1024]{1,0:T(8,128)(2,1)S(1)} collective-permute-done((bf16[64,1024]{1,0:T(8,128)(2,1)}, bf16[64,1024]{1,0:T(8,128)(2,1)S(1)}, u32[]{:S(2)}, u32[]{:S(2)}) %collective-permute-start) | collective-permute-done | bytes 131104 | tf_op jit(solution)/shard_map/ppermute | solution.py:198
  54.7 1.5 collective-permute-start.19
  56.3 0.9 fusion.19
  57.2 2.1 %collective-permute-start.1 = (bf16[2,64,1024]{2,1,0:T(8,128)(2,1)S(1)}, bf16[2,64,1024]{2,1,0:T(8,128)(2,1)S(1)}, u32[]{:S(2)}, u32[]{:S(2)}) collective-permute-start(bf16[2,64,1024]{2,1,0:T(8,128)(2,1)S(1)} %get-tuple-element.37), channel_id=1, source_target_pairs={{0,8},{4,12},{8,0},{12,4},{16,24},{20,28},{24,16},{28,20},{1,9},{5... | collective-permute-start | bytes 786440 | tf_op jit(solution)/shard_map/ppermute | solution.py:198
  59.5 7.2 %collective-permute-done.1 = bf16[2,64,1024]{2,1,0:T(8,128)(2,1)S(1)} collective-permute-done((bf16[2,64,1024]{2,1,0:T(8,128)(2,1)S(1)}, bf16[2,64,1024]{2,1,0:T(8,128)(2,1)S(1)}, u32[]{:S(2)}, u32[]{:S(2)}) %collective-permute-start.1) | collective-permute-done | bytes 262176 | tf_op jit(solution)/shard_map/ppermute | solution.py:198
  67.2 0.9 fusion.21
  68.0 17.8 %collective-permute-done.4 = bf16[2,64,1152]{2,1,0:T(8,128)(2,1)S(1)} collective-permute-done((bf16[2,64,1152]{2,1,0:T(8,128)(2,1)S(1)}, bf16[2,64,1152]{2,1,0:T(8,128)(2,1)S(1)}, u32[]{:S(2)}, u32[]{:S(2)}) %collective-permute-start.4) | collective-permute-done | bytes 294944 | tf_op jit(solution)/shard_map/ppermute | solution.py:198
  85.9 1.0 fusion.22
  86.9 0.9 collective-permute-start.5
  87.8 1.8 %mixer_finish.1 = bf16[512,2048]{1,0:T(8,128)(2,1)S(1)} custom-call(f32[512,256]{1,0:T(8,128)S(1)} %copy-done.10, bf16[512,256]{1,0:T(8,128)(2,1)S(1)} %get-tuple-element.13.query_ref, bf16[7,80,256]{2,1,0:T(8,128)(2,1)S(1)} %bitcast_dynamic-update-slice_fusion.all_ref, f32[1,256]{1,0:T(1,128)S(1)} %bitcast.133, bf16[256,2048]{1,0:T(8,128)(2,1)S(1)} %copy-done.5), custom_call_target="tpu_custom_call" | custom-call | flops 4000000000 | bytes 5000000 | tf_op jit(solution)/shard_map/mixer_finish/pallas_call | solution.py:179
  89.6 19.2 %collective-permute-done.26.refs_4_ = bf16[256,1024]{1,0:T(8,128)(2,1)} collective-permute-done((bf16[256,1024]{1,0:T(8,128)(2,1)}, bf16[256,1024]{1,0:T(8,128)(2,1)}, u32[]{:S(2)}, u32[]{:S(2)}) %collective-permute-start.26) | collective-permute-done | bytes 524320 | tf_op jit(solution)/shard_map/ppermute | solution.py:198
  109.3 1.1 dynamic-slice_bitcast_fusion
  110.4 0.9 copy-done.15
  111.4 1.4 fusion.8
  113.4 1.3 pad_maximum_fusion.1
  115.5 1.5 collective-permute-start.22
  117.0 1.6 fusion.3
  118.6 4.8 %expert_units.2.refs_0_ = bf16[512,512]{1,0:T(8,128)(2,1)S(1)} custom-call(bf16[512,1024]{1,0:T(8,128)(2,1)S(1)} %bitcast.129, bf16[512,1152]{1,0:T(8,128)(2,1)S(1)} %bitcast.120, bf16[2048,256]{1,0:T(8,128)(2,1)} %bitcast.32.refs_0_, bf16[2048,256]{1,0:T(8,128)(2,1)} %collective-permute-done.15.refs_1_, bf16[2048,256]{1,0:T(8,128)(2,1)} %bitcast.33.refs_2_, ...), custom_call_target="tpu_custom_call" | custom-call | flops 2147483648 | bytes 6291456 | tf_op jit(solution)/shard_map/expert_units/pallas_call | solution.py:289
  123.4 6.0 %collective-permute-done.22.refs_4_ = bf16[256,1024]{1,0:T(8,128)(2,1)S(1)} collective-permute-done((bf16[256,1024]{1,0:T(8,128)(2,1)S(1)}, bf16[256,1024]{1,0:T(8,128)(2,1)S(1)}, u32[]{:S(2)}, u32[]{:S(2)}) %collective-permute-start.22) | collective-permute-done | bytes 524320 | tf_op jit(solution)/shard_map/ppermute | solution.py:198
  129.9 4.2 %expert_units.3.refs_1_ = bf16[512,512]{1,0:T(8,128)(2,1)S(1)} custom-call(bf16[512,1024]{1,0:T(8,128)(2,1)S(1)} %bitcast.130, bf16[512,1152]{1,0:T(8,128)(2,1)S(1)} %bitcast.121, bf16[2048,256]{1,0:T(8,128)(2,1)} %collective-permute-done.17.refs_0_, bf16[2048,256]{1,0:T(8,128)(2,1)S(1)} %collective-permute-done.18.refs_1_, ...), custom_call_target="tpu_custom_call" | custom-call | flops 2147483648 | bytes 6291456 | tf_op jit(solution)/shard_map/expert_units/pallas_call | solution.py:289
  134.1 2.7 %expert_rows.3 = bf16[512,1024]{1,0:T(8,128)(2,1)S(1)} custom-call(s32[1]{0:T(128)} %bitcast.place_ref, bf16[512,1152]{1,0:T(8,128)(2,1)S(1)} %bitcast.122, bf16[512,512]{1,0:T(8,128)(2,1)S(1)} %expert_units.2.refs_0_, bf16[512,512]{1,0:T(8,128)(2,1)S(1)} %expert_units.3.refs_1_, bf16[256,1024]{1,0:T(8,128)(2,1)} %get-tuple-element.26.refs_2_, ...), custom_call_target="tpu_custom_call" | custom-call | flops 1073741824 | bytes 8000000 | tf_op jit(solution)/shard_map/expert_rows/pallas_call | solution.py:326
  136.9 1.2 collective-permute-start.28
  138.1 1.5 expert_rows.2
  139.7 1.6 collective-permute-start.34
  141.3 2.1 %collective-permute-start.31 = (bf16[2,2,64,1024]{3,2,1,0:T(8,128)(2,1)S(1)}, bf16[2,2,64,1024]{3,2,1,0:T(8,128)(2,1)S(1)}, u32[]{:S(2)}, u32[]{:S(2)}) collective-permute-start(bf16[2,2,64,1024]{3,2,1,0:T(8,128)(2,1)S(1)} %slice_bitcast_fusion), channel_id=1, source_target_pairs={{0,8},{4,12},{8,0},{12,4},{16,24},{20,28},{24,16},{28,20},{1,9},{5... | collective-permute-start | bytes 1572872 | tf_op jit(solution)/shard_map/ppermute | solution.py:198
  143.4 0.6 collective-permute-start.24
  144.0 6.9 %collective-permute-done.28 = bf16[2,2,64,1024]{3,2,0,1:T(8,128)(2,1)S(1)} collective-permute-done((bf16[2,2,64,1024]{3,2,0,1:T(8,128)(2,1)S(1)}, bf16[2,2,64,1024]{3,2,0,1:T(8,128)(2,1)S(1)}, u32[]{:S(2)}, u32[]{:S(2)}) %collective-permute-start.28) | collective-permute-done | bytes 524320 | tf_op jit(solution)/shard_map/ppermute | solution.py:198
  151.1 2.1 %collective-permute-start.29 = (bf16[2,64,1024]{2,1,0:T(8,128)(2,1)S(1)}, bf16[2,64,1024]{2,1,0:T(8,128)(2,1)S(1)}, u32[]{:S(2)}, u32[]{:S(2)}) collective-permute-start(bf16[2,64,1024]{2,1,0:T(8,128)(2,1)S(1)} %slice_bitcast_fusion.4), channel_id=1, source_target_pairs={{0,8},{4,12},{8,0},{12,4},{16,24},{20,28},{24,16},{28,20},{1,9},{5... | collective-permute-start | bytes 786440 | tf_op jit(solution)/shard_map/ppermute | solution.py:198
  153.2 3.0 %collective-permute-done.31 = bf16[2,2,64,1024]{3,2,1,0:T(8,128)(2,1)S(1)} collective-permute-done((bf16[2,2,64,1024]{3,2,1,0:T(8,128)(2,1)S(1)}, bf16[2,2,64,1024]{3,2,1,0:T(8,128)(2,1)S(1)}, u32[]{:S(2)}, u32[]{:S(2)}) %collective-permute-start.31) | collective-permute-done | bytes 524320 | tf_op jit(solution)/shard_map/ppermute | solution.py:198
  156.4 2.5 %collective-permute-done.24 = bf16[128,2048]{1,0:T(8,128)(2,1)S(1)} collective-permute-done((bf16[128,2048]{1,0:T(8,128)(2,1)S(1)}, bf16[128,2048]{1,0:T(8,128)(2,1)S(1)}, u32[]{:S(2)}, u32[]{:S(2)}) %collective-permute-start.24) | collective-permute-done | bytes 524320 | tf_op jit(solution)/shard_map/ppermute | solution.py:198
  158.9 0.9 fusion.7
  159.8 2.8 %collective-permute-done.29 = bf16[2,64,1024]{2,1,0:T(8,128)(2,1)S(1)} collective-permute-done((bf16[2,64,1024]{2,1,0:T(8,128)(2,1)S(1)}, bf16[2,64,1024]{2,1,0:T(8,128)(2,1)S(1)}, u32[]{:S(2)}, u32[]{:S(2)}) %collective-permute-start.29) | collective-permute-done | bytes 262176 | tf_op jit(solution)/shard_map/ppermute | solution.py:198
  162.8 10.2 %collective-permute-done.32 = bf16[2,64,1024]{2,1,0:T(8,128)(2,1)S(1)} collective-permute-done((bf16[2,64,1024]{2,1,0:T(8,128)(2,1)S(1)}, bf16[2,64,1024]{2,1,0:T(8,128)(2,1)S(1)}, u32[]{:S(2)}, u32[]{:S(2)}) %collective-permute-start.32) | collective-permute-done | bytes 262176 | tf_op jit(solution)/shard_map/ppermute | solution.py:198
  173.0 0.6 collective-permute-start.33
  173.7 0.8 collective-permute-done.30
  174.5 3.6 %collective-permute-done.33 = bf16[64,1024]{1,0:T(8,128)(2,1)S(1)} collective-permute-done((bf16[64,1024]{1,0:T(8,128)(2,1)S(1)}, bf16[64,1024]{1,0:T(8,128)(2,1)S(1)}, u32[]{:S(2)}, u32[]{:S(2)}) %collective-permute-start.33) | collective-permute-done | bytes 131104 | tf_op jit(solution)/shard_map/ppermute | solution.py:198
  178.1 0.8 fusion.9
  (108 shorter events, 5.1 us)
Async XLA Ops:
  0.6 37.0 %copy-start = (bf16[128,2048]{1,0:T(8,128)(2,1)S(1)}, bf16[128,2048]{1,0:T(8,128)(2,1)}, u32[]{:S(2)}) copy-start(bf16[128,2048]{1,0:T(8,128)(2,1)} %param.37) | copy-start | bytes 1572868
  1.5 1.6 copy-start.1
  3.1 1.2 copy-start.2
  4.4 1.2 copy-start.3
  5.6 1.2 copy-start.4
  6.8 0.7 copy-start.6
  7.5 0.7 copy-start.7
  8.2 25.7 %copy-start.12 = (bf16[256,2048]{1,0:T(8,128)(2,1)S(1)}, bf16[256,2048]{1,0:T(8,128)(2,1)}, u32[]{:S(2)}) copy-start(bf16[256,2048]{1,0:T(8,128)(2,1)} %param.28) | copy-start | bytes 3145732
  8.2 26.0 %copy-start.20 = (f32[64,4]{0,1:T(4,128)S(1)}, f32[64,4]{0,1:T(4,128)}, u32[]{:S(2)}) copy-start(f32[64,4]{0,1:T(4,128)} %param.31) | copy-start | bytes 3076
  8.2 26.0 %copy-start.21 = (s32[256,4]{0,1:T(4,128)S(1)}, s32[256,4]{0,1:T(4,128)}, u32[]{:S(2)}) copy-start(s32[256,4]{0,1:T(4,128)} %param.30) | copy-start | bytes 12292
  8.2 26.1 %copy-start.14 = (bf16[1,256,2048]{2,1,0:T(8,128)(2,1)S(1)}, bf16[1,256,2048]{2,1,0:T(8,128)(2,1)}, u32[]{:S(2)}) copy-start(bf16[1,256,2048]{2,1,0:T(8,128)(2,1)} %param.34) | copy-start | bytes 3145732
  18.0 0.8 copy-start.9
  18.8 16.4 %copy-start.19 = (f32[2048]{0:T(1024)S(1)}, f32[2048]{0:T(1024)}, u32[]{:S(2)}) copy-start(f32[2048]{0:T(1024)} %param.29) | copy-start | bytes 24580
  18.8 23.6 %collective-permute-start.6 = (bf16[80,256]{1,0:T(8,128)(2,1)S(1)}, bf16[80,256]{1,0:T(8,128)(2,1)}, u32[]{:S(2)}, u32[]{:S(2)}) collective-permute-start(bf16[80,256]{1,0:T(8,128)(2,1)S(1)} %get-tuple-element.14), channel_id=1, source_target_pairs={{0,28},{1,29},{2,30},{3,31}} | collective-permute-start | bytes 122888 | tf_op jit(solution)/shard_map/ppermute | solution.py:267
  27.5 17.1 %collective-permute-start.7 = (bf16[80,256]{1,0:T(8,128)(2,1)S(1)}, bf16[80,256]{1,0:T(8,128)(2,1)}, u32[]{:S(2)}, u32[]{:S(2)}) collective-permute-start(bf16[80,256]{1,0:T(8,128)(2,1)S(1)} %get-tuple-element.14), channel_id=1, source_target_pairs={{0,24},{4,28},{1,25},{5,29},{2,26},{6,30},{3,27},{7,31}} | collective-permute-start | bytes 122888 | tf_op jit(solution)/shard_map/ppermute | solution.py:267
  29.3 18.5 %collective-permute-start.8 = (bf16[80,256]{1,0:T(8,128)(2,1)S(1)}, bf16[80,256]{1,0:T(8,128)(2,1)}, u32[]{:S(2)}, u32[]{:S(2)}) collective-permute-start(bf16[80,256]{1,0:T(8,128)(2,1)S(1)} %get-tuple-element.14), channel_id=1, source_target_pairs={{0,20},{4,24},{8,28},{1,21},{5,25},{9,29},{2,22},{6,26},{10,30},{3... | collective-permute-start | bytes 122888 | tf_op jit(solution)/shard_map/ppermute | solution.py:267
  31.3 17.3 %collective-permute-start.9 = (bf16[80,256]{1,0:T(8,128)(2,1)S(1)}, bf16[80,256]{1,0:T(8,128)(2,1)S(1)}, u32[]{:S(2)}, u32[]{:S(2)}) collective-permute-start(bf16[80,256]{1,0:T(8,128)(2,1)S(1)} %get-tuple-element.14), channel_id=1, source_target_pairs={{0,16},{4,20},{8,24},{12,28},{1,17},{5,21},{9,25},{13,29},{2,18},{... | collective-permute-start | bytes 122888 | tf_op jit(solution)/shard_map/ppermute | solution.py:267
  32.6 16.1 %collective-permute-start.10 = (bf16[80,256]{1,0:T(8,128)(2,1)S(1)}, bf16[80,256]{1,0:T(8,128)(2,1)S(1)}, u32[]{:S(2)}, u32[]{:S(2)}) collective-permute-start(bf16[80,256]{1,0:T(8,128)(2,1)S(1)} %get-tuple-element.14), channel_id=1, source_target_pairs={{0,12},{4,16},{8,20},{12,24},{16,28},{1,13},{5,17},{9,21},{13,25},... | collective-permute-start | bytes 122888 | tf_op jit(solution)/shard_map/ppermute | solution.py:267
  39.5 19.9 %copy-start.11 = (bf16[256,2048]{1,0:T(8,128)(2,1)}, bf16[256,2048]{1,0:T(8,128)(2,1)S(1)}, u32[]{:S(2)}) copy-start(bf16[256,2048]{1,0:T(8,128)(2,1)S(1)} %convolution_convert_fusion) | copy-start | bytes 3145732
  42.5 7.1 %collective-permute-start.11 = (bf16[80,256]{1,0:T(8,128)(2,1)S(1)}, bf16[80,256]{1,0:T(8,128)(2,1)S(1)}, u32[]{:S(2)}, u32[]{:S(2)}) collective-permute-start(bf16[80,256]{1,0:T(8,128)(2,1)S(1)} %get-tuple-element.14), channel_id=1, source_target_pairs={{0,8},{4,12},{8,16},{12,20},{16,24},{20,28},{1,9},{5,13},{9,17},{1... | collective-permute-start | bytes 122888 | tf_op jit(solution)/shard_map/ppermute | solution.py:267
  44.5 14.8 %collective-permute-start.12 = (bf16[80,256]{1,0:T(8,128)(2,1)S(1)}, bf16[80,256]{1,0:T(8,128)(2,1)S(1)}, u32[]{:S(2)}, u32[]{:S(2)}) collective-permute-start(bf16[80,256]{1,0:T(8,128)(2,1)S(1)} %get-tuple-element.14), channel_id=1, source_target_pairs={{0,4},{4,8},{8,12},{12,16},{16,20},{20,24},{24,28},{1,5},{5,9},{9,... | collective-permute-start | bytes 122888 | tf_op jit(solution)/shard_map/ppermute | solution.py:267
  47.8 9.4 %collective-permute-start.3 = (bf16[64,1152]{1,0:T(8,128)(2,1)S(1)}, bf16[64,1152]{1,0:T(8,128)(2,1)S(1)}, u32[]{:S(2)}, u32[]{:S(2)}) collective-permute-start(bf16[64,1152]{1,0:T(8,128)(2,1)S(1)} %concatenate.6), channel_id=1, source_target_pairs={{0,8},{4,12},{8,0},{12,4},{16,24},{20,28},{24,16},{28,20},{1,9},{5... | collective-permute-start | bytes 442376 | tf_op jit(solution)/shard_map/ppermute | solution.py:198
  48.6 38.3 %collective-permute-start.14 = (bf16[2,64,2048]{2,1,0:T(8,128)(2,1)}, bf16[2,64,2048]{2,1,0:T(8,128)(2,1)S(1)}, u32[]{:S(2)}, u32[]{:S(2)}) collective-permute-start(bf16[2,64,2048]{2,1,0:T(8,128)(2,1)} %dynamic-slice_bitcast_fusion.2), channel_id=1, source_target_pairs={{0,1},{1,0},{2,3},{3,2},{4,5},{5,4},{6,7},{7,6},{8,9},{9,8},{10,11... | collective-permute-start | bytes 1572872 | tf_op jit(solution)/shard_map/ppermute | solution.py:198
  48.6 6.1 %collective-permute-start = (bf16[64,1024]{1,0:T(8,128)(2,1)}, bf16[64,1024]{1,0:T(8,128)(2,1)S(1)}, u32[]{:S(2)}, u32[]{:S(2)}) collective-permute-start(bf16[64,1024]{1,0:T(8,128)(2,1)} %get-tuple-element.29), channel_id=1, source_target_pairs={{0,4},{4,0},{8,12},{12,8},{16,20},{20,16},{24,28},{28,24},{1,5},{5... | collective-permute-start | bytes 393224 | tf_op jit(solution)/shard_map/ppermute | solution.py:198
  49.6 63.2 %collective-permute-start.17 = (bf16[2048,256]{1,0:T(8,128)(2,1)}, bf16[2048,256]{1,0:T(8,128)(2,1)}, u32[]{:S(2)}, u32[]{:S(2)}) collective-permute-start(bf16[2048,256]{1,0:T(8,128)(2,1)} %bitcast.32.refs_0_), channel_id=1, source_target_pairs={{0,2},{1,3},{2,0},{3,1},{4,6},{5,7},{6,4},{7,5},{8,10},{9,11},{10,... | collective-permute-start | bytes 3145736 | tf_op jit(solution)/shard_map/ppermute | solution.py:198
  54.7 58.6 %collective-permute-start.19 = (bf16[2048,256]{1,0:T(8,128)(2,1)}, bf16[2048,256]{1,0:T(8,128)(2,1)}, u32[]{:S(2)}, u32[]{:S(2)}) collective-permute-start(bf16[2048,256]{1,0:T(8,128)(2,1)} %bitcast.33.refs_2_), channel_id=1, source_target_pairs={{0,2},{1,3},{2,0},{3,1},{4,6},{5,7},{6,4},{7,5},{8,10},{9,11},{10,... | collective-permute-start | bytes 3145736 | tf_op jit(solution)/shard_map/ppermute | solution.py:198
  57.2 9.4 %collective-permute-start.1 = (bf16[2,64,1024]{2,1,0:T(8,128)(2,1)S(1)}, bf16[2,64,1024]{2,1,0:T(8,128)(2,1)S(1)}, u32[]{:S(2)}, u32[]{:S(2)}) collective-permute-start(bf16[2,64,1024]{2,1,0:T(8,128)(2,1)S(1)} %get-tuple-element.37), channel_id=1, source_target_pairs={{0,8},{4,12},{8,0},{12,4},{16,24},{20,28},{24,16},{28,20},{1,9},{5... | collective-permute-start | bytes 786440 | tf_op jit(solution)/shard_map/ppermute | solution.py:198
  59.3 28.5 %copy-start.5 = (bf16[256,2048]{1,0:T(8,128)(2,1)S(1)}, bf16[256,2048]{1,0:T(8,128)(2,1)}, u32[]{:S(2)}) copy-start(bf16[256,2048]{1,0:T(8,128)(2,1)} %out_w_ref.1) | copy-start | bytes 3145732
  59.3 28.5 %copy-start.8 = (f32[256]{0:T(256)S(1)}, f32[256]{0:T(256)}, u32[]{:S(2)}) copy-start(f32[256]{0:T(256)} %param.26) | copy-start | bytes 3076
  59.3 28.5 %copy-start.10 = (f32[512,256]{1,0:T(8,128)S(1)}, f32[512,256]{1,0:T(8,128)}, u32[]{:S(2)}) copy-start(f32[512,256]{1,0:T(8,128)} %copy-done.9) | copy-start | bytes 1572868
  59.4 26.5 %collective-permute-start.4 = (bf16[2,64,1152]{2,1,0:T(8,128)(2,1)S(1)}, bf16[2,64,1152]{2,1,0:T(8,128)(2,1)S(1)}, u32[]{:S(2)}, u32[]{:S(2)}) collective-permute-start(bf16[2,64,1152]{2,1,0:T(8,128)(2,1)S(1)} %get-tuple-element.35), channel_id=1, source_target_pairs={{0,16},{4,20},{8,24},{12,28},{16,0},{20,4},{24,8},{28,12},{1,17},{... | collective-permute-start | bytes 884744 | tf_op jit(solution)/shard_map/ppermute | solution.py:198
  66.7 42.2 %collective-permute-start.26 = (bf16[256,1024]{1,0:T(8,128)(2,1)}, bf16[256,1024]{1,0:T(8,128)(2,1)}, u32[]{:S(2)}, u32[]{:S(2)}) collective-permute-start(bf16[256,1024]{1,0:T(8,128)(2,1)} %get-tuple-element.26.refs_2_), channel_id=1, source_target_pairs={{0,2},{1,3},{2,0},{3,1},{4,6},{5,7},{6,4},{7,5},{8,10},{9,11},{10,... | collective-permute-start | bytes 1572872 | tf_op jit(solution)/shard_map/ppermute | solution.py:198
  85.9 22.9 %collective-permute-start.2 = (bf16[2,2,64,1024]{3,2,1,0:T(8,128)(2,1)S(1)}, bf16[2,2,64,1024]{3,2,1,0:T(8,128)(2,1)S(1)}, u32[]{:S(2)}, u32[]{:S(2)}) collective-permute-start(bf16[2,2,64,1024]{3,2,1,0:T(8,128)(2,1)S(1)} %get-tuple-element.33), channel_id=1, source_target_pairs={{0,16},{4,20},{8,24},{12,28},{16,0},{20,4},{24,8},{28,12},{1,17},{... | collective-permute-start | bytes 1572872 | tf_op jit(solution)/shard_map/ppermute | solution.py:198
  86.9 0.9 copy-start.17
  86.9 23.5 %collective-permute-start.5 = (bf16[2,2,64,1152]{3,2,1,0:T(8,128)(2,1)S(1)}, bf16[2,2,64,1152]{3,2,1,0:T(8,128)(2,1)S(1)}, u32[]{:S(2)}, u32[]{:S(2)}) collective-permute-start(bf16[2,2,64,1152]{3,2,1,0:T(8,128)(2,1)S(1)} %get-tuple-element.31), channel_id=1, source_target_pairs={{0,4},{4,0},{8,12},{12,8},{16,20},{20,16},{24,28},{28,24},{1,5},{5... | collective-permute-start | bytes 1769480 | tf_op jit(solution)/shard_map/ppermute | solution.py:198
  108.8 6.2 %collective-permute-start.15 = (bf16[2048,256]{1,0:T(8,128)(2,1)}, bf16[2048,256]{1,0:T(8,128)(2,1)}, u32[]{:S(2)}, u32[]{:S(2)}) collective-permute-start(bf16[2048,256]{1,0:T(8,128)(2,1)} %bitcast.32.refs_0_), channel_id=1, source_target_pairs={{0,1},{1,0},{2,3},{3,2},{4,5},{5,4},{6,7},{7,6},{8,9},{9,8},{10,11... | collective-permute-start | bytes 3145736 | tf_op jit(solution)/shard_map/ppermute | solution.py:198
  108.8 1.6 copy-start.18
  108.8 6.6 %collective-permute-start.16 = (bf16[2048,256]{1,0:T(8,128)(2,1)}, bf16[2048,256]{1,0:T(8,128)(2,1)}, u32[]{:S(2)}, u32[]{:S(2)}) collective-permute-start(bf16[2048,256]{1,0:T(8,128)(2,1)} %bitcast.33.refs_2_), channel_id=1, source_target_pairs={{0,1},{1,0},{2,3},{3,2},{4,5},{5,4},{6,7},{7,6},{8,9},{9,8},{10,11... | collective-permute-start | bytes 3145736 | tf_op jit(solution)/shard_map/ppermute | solution.py:198
  110.4 0.9 copy-start.15
  111.3 5.7 %collective-permute-start.13 = (bf16[2,128,2048]{2,1,0:T(8,128)(2,1)}, bf16[2,128,2048]{2,1,0:T(8,128)(2,1)}, u32[]{:S(2)}, u32[]{:S(2)}) collective-permute-start(bf16[2,128,2048]{2,1,0:T(8,128)(2,1)} %dynamic-slice_bitcast_fusion), channel_id=1, source_target_pairs={{0,1},{1,0},{2,3},{3,2},{4,5},{5,4},{6,7},{7,6},{8,9},{9,8},{10,11... | collective-permute-start | bytes 3145736 | tf_op jit(solution)/shard_map/ppermute | solution.py:198
  111.4 3.3 %copy-start.13 = (bf16[2,2,1,64,1152]{4,3,1,0,2:T(8,128)(2,1)S(1)}, bf16[2,2,1,64,1152]{4,3,1,0,2:T(8,128)(2,1)}, u32[]{:S(2)}) copy-start(bf16[2,2,1,64,1152]{4,3,1,0,2:T(8,128)(2,1)} %get-tuple-element.30) | copy-start | bytes 1769476
  111.4 3.3 %copy-start.16 = (bf16[2,2,64,1152]{3,2,1,0:T(8,128)(2,1)S(1)}, bf16[2,2,64,1152]{3,2,1,0:T(8,128)(2,1)}, u32[]{:S(2)}) copy-start(bf16[2,2,64,1152]{3,2,1,0:T(8,128)(2,1)} %copy-done.15) | copy-start | bytes 1769476
  112.8 16.6 %collective-permute-start.18 = (bf16[2048,256]{1,0:T(8,128)(2,1)}, bf16[2048,256]{1,0:T(8,128)(2,1)S(1)}, u32[]{:S(2)}, u32[]{:S(2)}) collective-permute-start(bf16[2048,256]{1,0:T(8,128)(2,1)} %collective-permute-done.17.refs_0_), channel_id=1, source_target_pairs={{0,1},{1,0},{2,3},{3,2},{4,5},{5,4},{6,7},{7,6},{8,9},{9,8},{10,11... | collective-permute-start | bytes 3145736 | tf_op jit(solution)/shard_map/ppermute | solution.py:198
  113.3 16.6 %collective-permute-start.20 = (bf16[2048,256]{1,0:T(8,128)(2,1)}, bf16[2048,256]{1,0:T(8,128)(2,1)S(1)}, u32[]{:S(2)}, u32[]{:S(2)}) collective-permute-start(bf16[2048,256]{1,0:T(8,128)(2,1)} %collective-permute-done.19.refs_2_), channel_id=1, source_target_pairs={{0,1},{1,0},{2,3},{3,2},{4,5},{5,4},{6,7},{7,6},{8,9},{9,8},{10,11... | collective-permute-start | bytes 3145736 | tf_op jit(solution)/shard_map/ppermute | solution.py:198
  115.0 19.1 %collective-permute-start.25 = (bf16[256,1024]{1,0:T(8,128)(2,1)}, bf16[256,1024]{1,0:T(8,128)(2,1)S(1)}, u32[]{:S(2)}, u32[]{:S(2)}) collective-permute-start(bf16[256,1024]{1,0:T(8,128)(2,1)} %get-tuple-element.26.refs_2_), channel_id=1, source_target_pairs={{0,1},{1,0},{2,3},{3,2},{4,5},{5,4},{6,7},{7,6},{8,9},{9,8},{10,11... | collective-permute-start | bytes 1572872 | tf_op jit(solution)/shard_map/ppermute | solution.py:198
  115.5 13.9 %collective-permute-start.22 = (bf16[256,1024]{1,0:T(8,128)(2,1)S(1)}, bf16[256,1024]{1,0:T(8,128)(2,1)S(1)}, u32[]{:S(2)}, u32[]{:S(2)}) collective-permute-start(bf16[256,1024]{1,0:T(8,128)(2,1)S(1)} %get-tuple-element.27.refs_2_), channel_id=1, source_target_pairs={{0,2},{1,3},{2,0},{3,1},{4,6},{5,7},{6,4},{7,5},{8,10},{9,11},{10,... | collective-permute-start | bytes 1572872 | tf_op jit(solution)/shard_map/ppermute | solution.py:198
  117.0 17.1 %collective-permute-start.27 = (bf16[256,1024]{1,0:T(8,128)(2,1)}, bf16[256,1024]{1,0:T(8,128)(2,1)S(1)}, u32[]{:S(2)}, u32[]{:S(2)}) collective-permute-start(bf16[256,1024]{1,0:T(8,128)(2,1)} %collective-permute-done.26.refs_4_), channel_id=1, source_target_pairs={{0,1},{1,0},{2,3},{3,2},{4,5},{5,4},{6,7},{7,6},{8,9},{9,8},{10,11... | collective-permute-start | bytes 1572872 | tf_op jit(solution)/shard_map/ppermute | solution.py:198
  129.4 8.7 %collective-permute-start.21 = (bf16[256,1024]{1,0:T(8,128)(2,1)S(1)}, bf16[256,1024]{1,0:T(8,128)(2,1)S(1)}, u32[]{:S(2)}, u32[]{:S(2)}) collective-permute-start(bf16[256,1024]{1,0:T(8,128)(2,1)S(1)} %get-tuple-element.27.refs_2_), channel_id=1, source_target_pairs={{0,1},{1,0},{2,3},{3,2},{4,5},{5,4},{6,7},{7,6},{8,9},{9,8},{10,11... | collective-permute-start | bytes 1572872 | tf_op jit(solution)/shard_map/ppermute | solution.py:198
  129.4 8.7 %collective-permute-start.23 = (bf16[256,1024]{1,0:T(8,128)(2,1)S(1)}, bf16[256,1024]{1,0:T(8,128)(2,1)S(1)}, u32[]{:S(2)}, u32[]{:S(2)}) collective-permute-start(bf16[256,1024]{1,0:T(8,128)(2,1)S(1)} %collective-permute-done.22.refs_4_), channel_id=1, source_target_pairs={{0,1},{1,0},{2,3},{3,2},{4,5},{5,4},{6,7},{7,6},{8,9},{9,8},{10,11... | collective-permute-start | bytes 1572872 | tf_op jit(solution)/shard_map/ppermute | solution.py:198
  136.9 13.9 %collective-permute-start.28 = (bf16[2,2,64,1024]{3,2,0,1:T(8,128)(2,1)S(1)}, bf16[2,2,64,1024]{3,2,0,1:T(8,128)(2,1)S(1)}, u32[]{:S(2)}, u32[]{:S(2)}) collective-permute-start(bf16[2,2,64,1024]{3,2,0,1:T(8,128)(2,1)S(1)} %bitcast.139), channel_id=1, source_target_pairs={{0,4},{4,0},{8,12},{12,8},{16,20},{20,16},{24,28},{28,24},{1,5},{5... | collective-permute-start | bytes 1572872 | tf_op jit(solution)/shard_map/ppermute | solution.py:198
  139.7 38.4 %collective-permute-start.34 = (bf16[64,2048]{1,0:T(8,128)(2,1)S(1)}, bf16[64,2048]{1,0:T(8,128)(2,1)S(1)}, u32[]{:S(2)}, u32[]{:S(2)}) collective-permute-start(bf16[64,2048]{1,0:T(8,128)(2,1)S(1)} %dynamic-slice_bitcast_fusion.3), channel_id=1, source_target_pairs={{0,2},{1,3},{2,0},{3,1},{4,6},{5,7},{6,4},{7,5},{8,10},{9,11},{10,... | collective-permute-start | bytes 786440 | tf_op jit(solution)/shard_map/ppermute | solution.py:198
  141.3 14.9 %collective-permute-start.31 = (bf16[2,2,64,1024]{3,2,1,0:T(8,128)(2,1)S(1)}, bf16[2,2,64,1024]{3,2,1,0:T(8,128)(2,1)S(1)}, u32[]{:S(2)}, u32[]{:S(2)}) collective-permute-start(bf16[2,2,64,1024]{3,2,1,0:T(8,128)(2,1)S(1)} %slice_bitcast_fusion), channel_id=1, source_target_pairs={{0,8},{4,12},{8,0},{12,4},{16,24},{20,28},{24,16},{28,20},{1,9},{5... | collective-permute-start | bytes 1572872 | tf_op jit(solution)/shard_map/ppermute | solution.py:198
  143.4 15.5 %collective-permute-start.24 = (bf16[128,2048]{1,0:T(8,128)(2,1)S(1)}, bf16[128,2048]{1,0:T(8,128)(2,1)S(1)}, u32[]{:S(2)}, u32[]{:S(2)}) collective-permute-start(bf16[128,2048]{1,0:T(8,128)(2,1)S(1)} %dynamic-slice_bitcast_fusion.1), channel_id=1, source_target_pairs={{0,2},{1,3},{2,0},{3,1},{4,6},{5,7},{6,4},{7,5},{8,10},{9,11},{10,... | collective-permute-start | bytes 1572872 | tf_op jit(solution)/shard_map/ppermute | solution.py:198
  151.1 11.5 %collective-permute-start.29 = (bf16[2,64,1024]{2,1,0:T(8,128)(2,1)S(1)}, bf16[2,64,1024]{2,1,0:T(8,128)(2,1)S(1)}, u32[]{:S(2)}, u32[]{:S(2)}) collective-permute-start(bf16[2,64,1024]{2,1,0:T(8,128)(2,1)S(1)} %slice_bitcast_fusion.4), channel_id=1, source_target_pairs={{0,8},{4,12},{8,0},{12,4},{16,24},{20,28},{24,16},{28,20},{1,9},{5... | collective-permute-start | bytes 786440 | tf_op jit(solution)/shard_map/ppermute | solution.py:198
  156.4 16.6 %collective-permute-start.32 = (bf16[2,64,1024]{2,1,0:T(8,128)(2,1)S(1)}, bf16[2,64,1024]{2,1,0:T(8,128)(2,1)S(1)}, u32[]{:S(2)}, u32[]{:S(2)}) collective-permute-start(bf16[2,64,1024]{2,1,0:T(8,128)(2,1)S(1)} %slice_bitcast_fusion.2), channel_id=1, source_target_pairs={{0,16},{4,20},{8,24},{12,28},{16,0},{20,4},{24,8},{28,12},{1,17},{... | collective-permute-start | bytes 786440 | tf_op jit(solution)/shard_map/ppermute | solution.py:198
  162.7 11.7 %collective-permute-start.30 = (bf16[64,1024]{1,0:T(8,128)(2,1)S(1)}, bf16[64,1024]{1,0:T(8,128)(2,1)S(1)}, u32[]{:S(2)}, u32[]{:S(2)}) collective-permute-start(bf16[64,1024]{1,0:T(8,128)(2,1)S(1)} %slice_bitcast_fusion.8), channel_id=1, source_target_pairs={{0,16},{4,20},{8,24},{12,28},{16,0},{20,4},{24,8},{28,12},{1,17},{... | collective-permute-start | bytes 393224 | tf_op jit(solution)/shard_map/ppermute | solution.py:198
  173.0 5.0 %collective-permute-start.33 = (bf16[64,1024]{1,0:T(8,128)(2,1)S(1)}, bf16[64,1024]{1,0:T(8,128)(2,1)S(1)}, u32[]{:S(2)}, u32[]{:S(2)}) collective-permute-start(bf16[64,1024]{1,0:T(8,128)(2,1)S(1)} %slice_bitcast_fusion.6), channel_id=1, source_target_pairs={{0,4},{4,0},{8,12},{12,8},{16,20},{20,16},{24,28},{28,24},{1,5},{5... | collective-permute-start | bytes 393224 | tf_op jit(solution)/shard_map/ppermute | solution.py:198
where the time goes:
time: 180 us; the launch traced here: 179 us
  waiting for transfers between devices  83.5 us (46%)
  starting transfers between devices  38.3 us (21%)
  Pallas kernels  24.8 us (14%)
  local copies, waits for them, and re-layouts  16.9 us (9%)
  other arithmetic  10.2 us (6%)
  matrix products  3.98 us (2%)
    ppermute x28, waiting for transfers between devices, swap(): lax.ppermute(x, axis, [(i, i ^ bit) for i in range(lax.axis_size(axis))])  83.5 us
    ppermute x28, starting transfers between devices, swap(): lax.ppermute(x, axis, [(i, i ^ bit) for i in range(lax.axis_size(axis))])  19.6 us
    ppermute x7, starting transfers between devices, carried_blocks(): lax.ppermute(carry, 'ep', [(i, i + d) for i in range(count - d)])  18.8 us
    unnamed x51, local copies, waits for them, and re-layouts  10.8 us
    pallas_call x1, Pallas kernels, mixer_scan(): pl.pallas_call(local_scan, grid=(rows // SPAN,), in_specs=[by_span(mix_in...  9.82 us
    pallas_call x2, Pallas kernels, expert_units(): pl.pallas_call(hidden_units, grid=(rows // block,), in_specs=[pl.BlockSpe...  8.98 us
    another operation x6, other arithmetic, gather_rows(): x = jnp.stack([x, swap(x, axis, bit)], axis=at)  4.26 us
    pallas_call x2, Pallas kernels, expert_rows(): pl.pallas_call(functools.partial(weighted_rows, experts), grid=(rows // b...  4.17 us
  transfers between devices with their start and end apart: 35, of which 12 were waited for; matrix products, arithmetic and copies ran while one was open for 12% of the time, Pallas kernels for 8%

commit v1 on v0

--- a/solution.py
+++ b/solution.py
@@ -108,21 +108,22 @@
         carry_ref[HEAD:] = tail.astype(jnp.bfloat16)
 
 
-def finish(mixed_ref, query_ref, all_ref, gain_ref, out_w_ref, part_ref, start):
+def finish(mixed_ref, query_ref, gain_ref, out_w_ref, *refs):
+    part_ref, start = refs[-2:]
     width = mixed_ref.shape[1]
     heads = width // HEAD
     mask = head_mask(width, width)
 
     @pl.when(pl.program_id(0) == 0)
     def _():
-        def one(lap, state):
-            block = all_ref[lap].astype(jnp.float32)
+        def one(ref, lap, state):
+            block = ref[lap].astype(jnp.float32)
             total = block[HEAD : HEAD + 1] + block[HEAD + 1 : HEAD + 2]
             return total * state + block[:HEAD]
 
-        packed = lax.fori_loop(
-            0, all_ref.shape[0], one, jnp.zeros((HEAD, width), jnp.float32)
-        )
+        packed = jnp.zeros((HEAD, width), jnp.float32)
+        for ref in refs[:-2]:
+            packed = lax.fori_loop(0, ref.shape[0], functools.partial(one, ref), packed)
         whole = jnp.concatenate([packed] * heads, axis=0)
         start[...] = jnp.where(mask, whole, 0.0).astype(jnp.bfloat16)
 
@@ -181,8 +182,8 @@
         grid=(rows // block,),
         in_specs=[
             by_rows(width), by_rows(width),
-            whole_block(carried), whole_block(gain), whole_block(w_out),
-        ],
+            whole_block(gain), whole_block(w_out),
+        ] + [whole_block(c) for c in carried],
         out_specs=by_rows(w_out.shape[1]),
         out_shape=jax.ShapeDtypeStruct((rows, w_out.shape[1]), jnp.bfloat16),
         scratch_shapes=[pltpu.VMEM((width, width), jnp.bfloat16)],
@@ -191,7 +192,7 @@
             flops=4_000_000_000, bytes_accessed=5_000_000, transcendentals=0
         ),
         name="mixer_finish",
-    )(mixed, query, carried, gain, w_out)
+    )(mixed, query, gain, w_out, *carried)
 
 
 def swap(x, axis, bit):
@@ -229,7 +230,8 @@
     bits = []
     for bit in order:
         at = sum(b > bit for b in bits)
-        x = jnp.stack([x, swap(x, axis, bit)], axis=at)
+        other = swap(x, axis, bit)
+        x = jnp.stack([x, other], axis=at)
         bits = sorted(bits + [bit], reverse=True)
     return x.reshape(-1, x.shape[-1])
 
@@ -241,7 +243,9 @@
         at = bits.index(bit)
         part = part.astype(jnp.bfloat16)
         keep = lax.index_in_dim(part, 0, at, False).astype(jnp.float32)
-        part = keep + swap(lax.index_in_dim(part, 1, at, False), axis, bit).astype(jnp.float32)
+        send = lax.index_in_dim(part, 1, at, False)
+        other = swap(send, axis, bit)
+        part = keep + other.astype(jnp.float32)
         bits = [b for b in bits if b != bit]
     return part
 
@@ -261,13 +265,11 @@
     if count > 8:
         held = lax.all_gather(carry, "ep")
         before = jnp.arange(count)[:, None, None] < lax.axis_index("ep")
-        return jnp.where(before, held, jnp.zeros_like(held))
-    return jnp.stack(
-        [
-            lax.ppermute(carry, "ep", [(i, i + d) for i in range(count - d)])
-            for d in range(count - 1, 0, -1)
-        ]
-    )
+        return [jnp.where(before, held, jnp.zeros_like(held))]
+    return [
+        lax.ppermute(carry, "ep", [(i, i + d) for i in range(count - d)])[None]
+        for d in range(count - 1, 0, -1)
+    ]
 
 
 def hidden_units(left_ref, right_ref, *refs):
@@ -360,8 +362,9 @@
     flat = lambda w: w.reshape(w.shape[1:])
     gates, far_gates = gather_groups(flat(w_exp_gate))
     ups, far_ups = gather_groups(flat(w_exp_up))
-    left_downs = sum(gather_groups(flat(w_exp_down)[:, :half]), [])
-    right_downs = sum(gather_groups(flat(w_exp_down)[:, half:]), [])
+    cut = model // 8 * 5
+    left_downs = sum(gather_groups(flat(w_exp_down)[:, :cut]), [])
+    right_downs = sum(gather_groups(flat(w_exp_down)[:, cut:]), [])
 
     hidden = norm_rows(moe_in, moe_gain)
     chance = jax.nn.sigmoid(route_logit)
@@ -383,8 +386,9 @@
     )
     ep_bits = axis_bits("ep")
     turned = ep_bits[1:] + ep_bits[:1]
-    left_rows = gather_rows(own_rows[:, :half], "ep", ep_bits)
-    right_rows = gather_rows(sent, "ep", turned)
+    far_first = ep_bits[:0:-1]
+    left_rows = gather_rows(own_rows[:, :half], "ep", ep_bits[:1] + far_first)
+    right_rows = gather_rows(sent, "ep", far_first + ep_bits[:1])
 
     mixed, query, carry = mixer_scan(
         mix_in, forget_shift, mix_gain, w_query, w_forget, w_value, forget_room

time: 180 us -> 183 us (1.017)
  starting transfers between devices: 38.3 us -> 50 us
  waiting for transfers between devices: 83.5 us -> 78.2 us
  local copies, waits for them, and re-layouts: 16.9 us -> 12.7 us
  other arithmetic: 10.2 us -> 14 us
    ppermute x7, starting transfers between devices: 18.8 us -> 27.8 us  [carried_blocks(): lax.ppermute(carry, 'ep', [(i, i + d) for i in range(count - d)])[None]]
    ppermute x28, waiting for transfers between devices: 83.5 us -> 77.7 us  [swap(): lax.ppermute(x, axis, [(i, i ^ bit) for i in range(lax.axis_size(axis))])]
    unnamed x51 -> x41, local copies, waits for them, and re-layouts: 10.8 us -> 6.06 us
    ppermute x28, starting transfers between devices: 19.6 us -> 22.2 us  [swap(): lax.ppermute(x, axis, [(i, i ^ bit) for i in range(lax.axis_size(axis))])]
  transfers between devices with their start and end apart: 35 -> 35, of which waited for: 12 -> 11; matrix products, arithmetic and copies ran while one was open for 12% -> 9% of each run, Pallas kernels for 8% -> 13%
where the time goes in v1:
time: 183 us; the launch traced here: 182 us
  waiting for transfers between devices  78.2 us (43%)
  starting transfers between devices  50 us (27%)
  Pallas kernels  23.6 us (13%)
  other arithmetic  14 us (8%)
  local copies, waits for them, and re-layouts  12.7 us (7%)
  matrix products  2.16 us (1%)
    ppermute x28, waiting for transfers between devices, swap(): lax.ppermute(x, axis, [(i, i ^ bit) for i in range(lax.axis_size(axis))])  77.7 us
    ppermute x7, starting transfers between devices, carried_blocks(): lax.ppermute(carry, 'ep', [(i, i + d) for i in range(count - d)])[None]  27.8 us
    ppermute x28, starting transfers between devices, swap(): lax.ppermute(x, axis, [(i, i ^ bit) for i in range(lax.axis_size(axis))])  22.2 us
    pallas_call x1, Pallas kernels, mixer_scan(): pl.pallas_call(local_scan, grid=(rows // SPAN,), in_specs=[by_span(mix_in...  9.89 us
    pallas_call x2, Pallas kernels, expert_units(): pl.pallas_call(hidden_units, grid=(rows // block,), in_specs=[pl.BlockSpe...  8.98 us
    unnamed x41, local copies, waits for them, and re-layouts  6.06 us
    another operation x6, other arithmetic, gather_rows(): x = jnp.stack([x, other], axis=at)  4.36 us
  transfers between devices with their start and end apart: 35, of which 11 were waited for; matrix products, arithmetic and copies ran while one was open for 9% of the time, Pallas kernels for 13%

profile of v1, /device:TPU:0, one launch (start us, length us, event | category | flops | bytes accessed | tf_op | source)
XLA Modules:
  0.0 181.8 jit_solution(13057764870368131724)
XLA Ops:
  0.7 1.6 fusion
  2.3 0.7 divide_reduce_fusion
  3.0 0.7 divide_multiply_fusion
  3.7 0.8 constant_dynamic-slice_fusion.1
  4.7 1.6 fusion.2
  6.4 4.1 %collective-permute-start.3 = (bf16[64,1152]{1,0:T(8,128)(2,1)S(1)}, bf16[64,1152]{1,0:T(8,128)(2,1)}, u32[]{:S(2)}, u32[]{:S(2)}) collective-permute-start(bf16[64,1152]{1,0:T(8,128)(2,1)S(1)} %concatenate.6), channel_id=1, source_target_pairs={{0,16},{4,20},{8,24},{12,28},{16,0},{20,4},{24,8},{28,12},{1,17},{... | collective-permute-start | bytes 442376 | tf_op jit(solution)/shard_map/ppermute | solution.py:199
  10.5 1.5 collective-permute-start
  12.0 0.4 fusion.25
  12.5 1.7 convolution_convert_fusion
  14.2 2.0 %dynamic-slice_bitcast_fusion.2 = bf16[2,64,2048]{2,1,0:T(8,128)(2,1)} fusion(bf16[2,2,64,2048]{3,2,1,0:T(8,128)(2,1)} %bitcast.134, s32[]{:T(128)S(6)} %select_n.54), kind=kLoop, calls=%fused_computation.31 | loop fusion | bytes 1048580 | tf_op jit(solution)/shard_map/jit(dynamic_index_in_dim)/squeeze | solution.py:218
  16.9 0.8 collective-permute-done.3
  17.7 1.0 fusion.20
  18.6 0.9 collective-permute-start.4
  19.5 1.2 copy-done.5
  20.7 1.2 copy-done.6
  22.0 1.2 copy-done.7
  23.2 9.9 %mixer_scan.1 = (f32[512,256]{1,0:T(8,128)S(1)}, bf16[512,256]{1,0:T(8,128)(2,1)S(1)}, bf16[80,256]{1,0:T(8,128)(2,1)S(1)}) custom-call(bf16[512,2048]{1,0:T(8,128)(2,1)S(1)} %copy-done.4, f32[512,1]{1,0:T(8,128)S(1)} %copy.46.shift_ref, f32[1,2048]{1,0:T(1,128)S(1)} %bitcast.131, bf16[2048,256]{1,0:T(8,128)(2,1)S(1)} %copy-done.5, ...), custom_call_target="tpu_custom_call" | custom-call | flops 40000000000 | bytes 7000000 | tf_op jit(solution)/shard_map/mixer_scan/pallas_call | solution.py:147
  33.1 11.1 %collective-permute-start.6 = (bf16[80,256]{1,0:T(8,128)(2,1)S(1)}, bf16[80,256]{1,0:T(8,128)(2,1)S(1)}, u32[]{:S(2)}, u32[]{:S(2)}) collective-permute-start(bf16[80,256]{1,0:T(8,128)(2,1)S(1)} %get-tuple-element.14), channel_id=1, source_target_pairs={{0,28},{1,29},{2,30},{3,31}} | collective-permute-start | bytes 122888 | tf_op jit(solution)/shard_map/ppermute | solution.py:270
  44.2 1.3 collective-permute-start.7
  45.6 0.5 collective-permute-done.6
  46.1 1.3 collective-permute-start.8
  47.4 1.3 collective-permute-start.9
  48.7 0.9 fusion.21
  49.5 8.3 %collective-permute-start.10 = (bf16[80,256]{1,0:T(8,128)(2,1)S(1)}, bf16[80,256]{1,0:T(8,128)(2,1)S(1)}, u32[]{:S(2)}, u32[]{:S(2)}) collective-permute-start(bf16[80,256]{1,0:T(8,128)(2,1)S(1)} %get-tuple-element.14), channel_id=1, source_target_pairs={{0,12},{4,16},{8,20},{12,24},{16,28},{1,13},{5,17},{9,21},{13,25},... | collective-permute-start | bytes 122888 | tf_op jit(solution)/shard_map/ppermute | solution.py:270
  57.8 1.3 collective-permute-start.11
  59.1 3.3 %collective-permute-start.12 = (bf16[80,256]{1,0:T(8,128)(2,1)S(1)}, bf16[80,256]{1,0:T(8,128)(2,1)S(1)}, u32[]{:S(2)}, u32[]{:S(2)}) collective-permute-start(bf16[80,256]{1,0:T(8,128)(2,1)S(1)} %get-tuple-element.14), channel_id=1, source_target_pairs={{0,4},{4,8},{8,12},{12,16},{16,20},{20,24},{24,28},{1,5},{5,9},{9,... | collective-permute-start | bytes 122888 | tf_op jit(solution)/shard_map/ppermute | solution.py:270
  62.4 1.6 collective-permute-start.26
  64.0 1.0 fusion.22
  65.0 0.5 collective-permute-start.17
  65.5 1.5 collective-permute-start.19
  67.0 0.9 collective-permute-start.5
  67.9 1.8 mixer_finish.1
  69.7 1.1 dynamic-slice_bitcast_fusion
  70.8 9.3 %collective-permute-done.26.refs_4_ = bf16[256,1280]{1,0:T(8,128)(2,1)S(1)} collective-permute-done((bf16[256,1280]{1,0:T(8,128)(2,1)S(1)}, bf16[256,1280]{1,0:T(8,128)(2,1)S(1)}, u32[]{:S(2)}, u32[]{:S(2)}) %collective-permute-start.26) | collective-permute-done | bytes 655392 | tf_op jit(solution)/shard_map/ppermute | solution.py:199
  80.1 0.9 copy-done.2
  81.0 0.5 collective-permute-start.16
  81.8 0.8 copy-done.14
  82.7 0.5 collective-permute-start.13
  83.2 1.8 slice.64.refs_2_
  85.0 1.3 fusion.7
  86.3 16.4 %collective-permute-done.17.refs_0_ = bf16[2048,256]{1,0:T(8,128)(2,1)} collective-permute-done((bf16[2048,256]{1,0:T(8,128)(2,1)}, bf16[2048,256]{1,0:T(8,128)(2,1)}, u32[]{:S(2)}, u32[]{:S(2)}) %collective-permute-start.17) | collective-permute-done | bytes 1048608 | tf_op jit(solution)/shard_map/ppermute | solution.py:199
  102.7 18.9 %collective-permute-done.19.refs_2_ = bf16[2048,256]{1,0:T(8,128)(2,1)} collective-permute-done((bf16[2048,256]{1,0:T(8,128)(2,1)}, bf16[2048,256]{1,0:T(8,128)(2,1)}, u32[]{:S(2)}, u32[]{:S(2)}) %collective-permute-start.19) | collective-permute-done | bytes 1048608 | tf_op jit(solution)/shard_map/ppermute | solution.py:199
  121.5 1.4 pad_maximum_fusion.1
  123.3 0.6 collective-permute-start.25
  124.1 1.5 collective-permute-start.22
  125.8 1.6 fusion.3
  127.5 4.8 %expert_units.2.refs_0_ = bf16[512,512]{1,0:T(8,128)(2,1)S(1)} custom-call(bf16[512,1024]{1,0:T(8,128)(2,1)S(1)} %bitcast.122, bf16[512,1152]{1,0:T(8,128)(2,1)S(1)} %bitcast.113, bf16[2048,256]{1,0:T(8,128)(2,1)} %bitcast.32.refs_0_, bf16[2048,256]{1,0:T(8,128)(2,1)} %collective-permute-done.15.refs_1_, bf16[2048,256]{1,0:T(8,128)(2,1)} %bitcast.33.refs_2_, ...), custom_call_target="tpu_custom_call" | custom-call | flops 2147483648 | bytes 6291456 | tf_op jit(solution)/shard_map/expert_units/pallas_call | solution.py:291
  132.3 3.3 %collective-permute-done.22.refs_4_ = bf16[256,768]{1,0:T(8,128)(2,1)S(1)} collective-permute-done((bf16[256,768]{1,0:T(8,128)(2,1)S(1)}, bf16[256,768]{1,0:T(8,128)(2,1)S(1)}, u32[]{:S(2)}, u32[]{:S(2)}) %collective-permute-start.22) | collective-permute-done | bytes 393248 | tf_op jit(solution)/shard_map/ppermute | solution.py:199
  135.6 0.5 collective-permute-start.23
  136.1 4.2 %expert_units.3.refs_1_ = bf16[512,512]{1,0:T(8,128)(2,1)S(1)} custom-call(bf16[512,1024]{1,0:T(8,128)(2,1)S(1)} %bitcast.123, bf16[512,1152]{1,0:T(8,128)(2,1)S(1)} %bitcast.114, bf16[2048,256]{1,0:T(8,128)(2,1)} %collective-permute-done.17.refs_0_, bf16[2048,256]{1,0:T(8,128)(2,1)S(1)} %collective-permute-done.18.refs_1_, ...), custom_call_target="tpu_custom_call" | custom-call | flops 2147483648 | bytes 6291456 | tf_op jit(solution)/shard_map/expert_units/pallas_call | solution.py:291
  140.3 1.8 expert_rows.3
  142.3 0.9 collective-permute-start.28
  143.2 1.2 expert_rows.2
  144.9 1.6 collective-permute-start.24
  146.5 0.6 collective-permute-start.34
  147.0 8.2 %collective-permute-done.31 = bf16[2,2,64,768]{3,2,1,0:T(8,128)(2,1)S(1)} collective-permute-done((bf16[2,2,64,768]{3,2,1,0:T(8,128)(2,1)S(1)}, bf16[2,2,64,768]{3,2,1,0:T(8,128)(2,1)S(1)}, u32[]{:S(2)}, u32[]{:S(2)}) %collective-permute-start.31) | collective-permute-done | bytes 393248 | tf_op jit(solution)/shard_map/ppermute | solution.py:199
  155.7 4.0 %collective-permute-done.24 = bf16[128,2048]{1,0:T(8,128)(2,1)S(1)} collective-permute-done((bf16[128,2048]{1,0:T(8,128)(2,1)S(1)}, bf16[128,2048]{1,0:T(8,128)(2,1)S(1)}, u32[]{:S(2)}, u32[]{:S(2)}) %collective-permute-start.24) | collective-permute-done | bytes 524320 | tf_op jit(solution)/shard_map/ppermute | solution.py:199
  159.7 0.9 fusion.6
  160.8 1.8 collective-permute-start.29
  162.6 3.5 %collective-permute-done.32 = bf16[2,64,768]{2,1,0:T(8,128)(2,1)S(1)} collective-permute-done((bf16[2,64,768]{2,1,0:T(8,128)(2,1)S(1)}, bf16[2,64,768]{2,1,0:T(8,128)(2,1)S(1)}, u32[]{:S(2)}, u32[]{:S(2)}) %collective-permute-start.32) | collective-permute-done | bytes 196640 | tf_op jit(solution)/shard_map/ppermute | solution.py:199
  166.2 1.3 collective-permute-start.33
  167.4 4.7 %collective-permute-done.29 = bf16[2,64,1280]{2,1,0:T(8,128)(2,1)S(1)} collective-permute-done((bf16[2,64,1280]{2,1,0:T(8,128)(2,1)S(1)}, bf16[2,64,1280]{2,1,0:T(8,128)(2,1)S(1)}, u32[]{:S(2)}, u32[]{:S(2)}) %collective-permute-start.29) | collective-permute-done | bytes 327712 | tf_op jit(solution)/shard_map/ppermute | solution.py:199
  172.4 8.6 %collective-permute-done.30 = bf16[64,1280]{1,0:T(8,128)(2,1)S(1)} collective-permute-done((bf16[64,1280]{1,0:T(8,128)(2,1)S(1)}, bf16[64,1280]{1,0:T(8,128)(2,1)S(1)}, u32[]{:S(2)}, u32[]{:S(2)}) %collective-permute-start.30) | collective-permute-done | bytes 163872 | tf_op jit(solution)/shard_map/ppermute | solution.py:199
  181.0 0.8 fusion.10
  (99 shorter events, 3.7 us)
Async XLA Ops:
  0.6 11.8 %copy-start = (bf16[128,2048]{1,0:T(8,128)(2,1)S(1)}, bf16[128,2048]{1,0:T(8,128)(2,1)}, u32[]{:S(2)}) copy-start(bf16[128,2048]{1,0:T(8,128)(2,1)} %param.37) | copy-start | bytes 1572868
  0.6 11.4 %copy-start.17 = (bf16[2048,128]{1,0:T(8,128)(2,1)S(1)}, bf16[2048,128]{1,0:T(8,128)(2,1)}, u32[]{:S(2)}) copy-start(bf16[2048,128]{1,0:T(8,128)(2,1)} %param.35) | copy-start | bytes 1572868
  4.7 7.8 %copy-start.16 = (bf16[2048,128]{1,0:T(8,128)(2,1)S(1)}, bf16[2048,128]{1,0:T(8,128)(2,1)}, u32[]{:S(2)}) copy-start(bf16[2048,128]{1,0:T(8,128)(2,1)} %param.36) | copy-start | bytes 1572868
  6.4 11.2 %collective-permute-start.3 = (bf16[64,1152]{1,0:T(8,128)(2,1)S(1)}, bf16[64,1152]{1,0:T(8,128)(2,1)}, u32[]{:S(2)}, u32[]{:S(2)}) collective-permute-start(bf16[64,1152]{1,0:T(8,128)(2,1)S(1)} %concatenate.6), channel_id=1, source_target_pairs={{0,16},{4,20},{8,24},{12,28},{16,0},{20,4},{24,8},{28,12},{1,17},{... | collective-permute-start | bytes 442376 | tf_op jit(solution)/shard_map/ppermute | solution.py:199
  10.5 5.9 %collective-permute-start = (bf16[64,1024]{1,0:T(8,128)(2,1)S(1)}, bf16[64,1024]{1,0:T(8,128)(2,1)S(1)}, u32[]{:S(2)}, u32[]{:S(2)}) collective-permute-start(bf16[64,1024]{1,0:T(8,128)(2,1)S(1)} %get-tuple-element.27), channel_id=1, source_target_pairs={{0,4},{4,0},{8,12},{12,8},{16,20},{20,16},{24,28},{28,24},{1,5},{5... | collective-permute-start | bytes 393224 | tf_op jit(solution)/shard_map/ppermute | solution.py:199
  12.5 3.8 %copy-start.19 = (f32[512]{0:T(512)S(1)}, f32[512]{0:T(512)}, u32[]{:S(2)}) copy-start(f32[512]{0:T(512)} %param.20) | copy-start | bytes 6148
  14.2 5.3 %copy-start.4 = (bf16[512,2048]{1,0:T(8,128)(2,1)S(1)}, bf16[512,2048]{1,0:T(8,128)(2,1)}, u32[]{:S(2)}) copy-start(bf16[512,2048]{1,0:T(8,128)(2,1)} %x_ref.1) | copy-start | bytes 6291460
  14.2 5.3 %copy-start.9 = (f32[2048]{0:T(1024)S(1)}, f32[2048]{0:T(1024)}, u32[]{:S(2)}) copy-start(f32[2048]{0:T(1024)} %param.21) | copy-start | bytes 24580
  14.2 5.3 %copy-start.10 = (f32[256]{0:T(256)S(1)}, f32[256]{0:T(256)}, u32[]{:S(2)}) copy-start(f32[256]{0:T(256)} %param.25) | copy-start | bytes 3076
  16.3 50.8 %collective-permute-start.14 = (bf16[2,64,2048]{2,1,0:T(8,128)(2,1)}, bf16[2,64,2048]{2,1,0:T(8,128)(2,1)}, u32[]{:S(2)}, u32[]{:S(2)}) collective-permute-start(bf16[2,64,2048]{2,1,0:T(8,128)(2,1)} %dynamic-slice_bitcast_fusion.2), channel_id=1, source_target_pairs={{0,1},{1,0},{2,3},{3,2},{4,5},{5,4},{6,7},{7,6},{8,9},{9,8},{10,11... | collective-permute-start | bytes 1572872 | tf_op jit(solution)/shard_map/ppermute | solution.py:199
  16.5 30.9 %collective-permute-start.1 = (bf16[2,64,1024]{2,1,0:T(8,128)(2,1)S(1)}, bf16[2,64,1024]{2,1,0:T(8,128)(2,1)S(1)}, u32[]{:S(2)}, u32[]{:S(2)}) collective-permute-start(bf16[2,64,1024]{2,1,0:T(8,128)(2,1)S(1)} %get-tuple-element.35), channel_id=1, source_target_pairs={{0,16},{4,20},{8,24},{12,28},{16,0},{20,4},{24,8},{28,12},{1,17},{... | collective-permute-start | bytes 786440 | tf_op jit(solution)/shard_map/ppermute | solution.py:199
  18.6 43.8 %collective-permute-start.4 = (bf16[2,64,1152]{2,1,0:T(8,128)(2,1)S(1)}, bf16[2,64,1152]{2,1,0:T(8,128)(2,1)S(1)}, u32[]{:S(2)}, u32[]{:S(2)}) collective-permute-start(bf16[2,64,1152]{2,1,0:T(8,128)(2,1)S(1)} %get-tuple-element.33), channel_id=1, source_target_pairs={{0,8},{4,12},{8,0},{12,4},{16,24},{20,28},{24,16},{28,20},{1,9},{5... | collective-permute-start | bytes 884744 | tf_op jit(solution)/shard_map/ppermute | solution.py:199
  19.5 1.2 copy-start.5
  20.7 1.2 copy-start.6
  22.0 1.2 copy-start.7
  23.2 22.3 %copy-start.13 = (bf16[1,256,2048]{2,1,0:T(8,128)(2,1)S(1)}, bf16[1,256,2048]{2,1,0:T(8,128)(2,1)}, u32[]{:S(2)}) copy-start(bf16[1,256,2048]{2,1,0:T(8,128)(2,1)} %param.34) | copy-start | bytes 3145732
  33.1 13.0 %collective-permute-start.6 = (bf16[80,256]{1,0:T(8,128)(2,1)S(1)}, bf16[80,256]{1,0:T(8,128)(2,1)S(1)}, u32[]{:S(2)}, u32[]{:S(2)}) collective-permute-start(bf16[80,256]{1,0:T(8,128)(2,1)S(1)} %get-tuple-element.14), channel_id=1, source_target_pairs={{0,28},{1,29},{2,30},{3,31}} | collective-permute-start | bytes 122888 | tf_op jit(solution)/shard_map/ppermute | solution.py:270
  44.2 5.3 %collective-permute-start.7 = (bf16[80,256]{1,0:T(8,128)(2,1)S(1)}, bf16[80,256]{1,0:T(8,128)(2,1)S(1)}, u32[]{:S(2)}, u32[]{:S(2)}) collective-permute-start(bf16[80,256]{1,0:T(8,128)(2,1)S(1)} %get-tuple-element.14), channel_id=1, source_target_pairs={{0,24},{4,28},{1,25},{5,29},{2,26},{6,30},{3,27},{7,31}} | collective-permute-start | bytes 122888 | tf_op jit(solution)/shard_map/ppermute | solution.py:270
  45.5 22.4 %copy-start.8 = (bf16[256,2048]{1,0:T(8,128)(2,1)S(1)}, bf16[256,2048]{1,0:T(8,128)(2,1)}, u32[]{:S(2)}) copy-start(bf16[256,2048]{1,0:T(8,128)(2,1)} %out_w_ref.1) | copy-start | bytes 3145732
  45.5 22.4 %copy-start.11 = (f32[256]{0:T(256)S(1)}, f32[256]{0:T(256)}, u32[]{:S(2)}) copy-start(f32[256]{0:T(256)} %param.26) | copy-start | bytes 3076
  46.1 11.7 %collective-permute-start.8 = (bf16[80,256]{1,0:T(8,128)(2,1)S(1)}, bf16[80,256]{1,0:T(8,128)(2,1)S(1)}, u32[]{:S(2)}, u32[]{:S(2)}) collective-permute-start(bf16[80,256]{1,0:T(8,128)(2,1)S(1)} %get-tuple-element.14), channel_id=1, source_target_pairs={{0,20},{4,24},{8,28},{1,21},{5,25},{9,29},{2,22},{6,26},{10,30},{3... | collective-permute-start | bytes 122888 | tf_op jit(solution)/shard_map/ppermute | solution.py:270
  47.4 11.7 %collective-permute-start.9 = (bf16[80,256]{1,0:T(8,128)(2,1)S(1)}, bf16[80,256]{1,0:T(8,128)(2,1)S(1)}, u32[]{:S(2)}, u32[]{:S(2)}) collective-permute-start(bf16[80,256]{1,0:T(8,128)(2,1)S(1)} %get-tuple-element.14), channel_id=1, source_target_pairs={{0,16},{4,20},{8,24},{12,28},{1,17},{5,21},{9,25},{13,29},{2,18},{... | collective-permute-start | bytes 122888 | tf_op jit(solution)/shard_map/ppermute | solution.py:270
  49.5 15.4 %collective-permute-start.10 = (bf16[80,256]{1,0:T(8,128)(2,1)S(1)}, bf16[80,256]{1,0:T(8,128)(2,1)S(1)}, u32[]{:S(2)}, u32[]{:S(2)}) collective-permute-start(bf16[80,256]{1,0:T(8,128)(2,1)S(1)} %get-tuple-element.14), channel_id=1, source_target_pairs={{0,12},{4,16},{8,20},{12,24},{16,28},{1,13},{5,17},{9,21},{13,25},... | collective-permute-start | bytes 122888 | tf_op jit(solution)/shard_map/ppermute | solution.py:270
  57.8 7.7 %collective-permute-start.11 = (bf16[80,256]{1,0:T(8,128)(2,1)S(1)}, bf16[80,256]{1,0:T(8,128)(2,1)S(1)}, u32[]{:S(2)}, u32[]{:S(2)}) collective-permute-start(bf16[80,256]{1,0:T(8,128)(2,1)S(1)} %get-tuple-element.14), channel_id=1, source_target_pairs={{0,8},{4,12},{8,16},{12,20},{16,24},{20,28},{1,9},{5,13},{9,17},{1... | collective-permute-start | bytes 122888 | tf_op jit(solution)/shard_map/ppermute | solution.py:270
  59.1 7.9 %collective-permute-start.12 = (bf16[80,256]{1,0:T(8,128)(2,1)S(1)}, bf16[80,256]{1,0:T(8,128)(2,1)S(1)}, u32[]{:S(2)}, u32[]{:S(2)}) collective-permute-start(bf16[80,256]{1,0:T(8,128)(2,1)S(1)} %get-tuple-element.14), channel_id=1, source_target_pairs={{0,4},{4,8},{8,12},{12,16},{16,20},{20,24},{24,28},{1,5},{5,9},{9,... | collective-permute-start | bytes 122888 | tf_op jit(solution)/shard_map/ppermute | solution.py:270
  62.4 17.7 %collective-permute-start.26 = (bf16[256,1280]{1,0:T(8,128)(2,1)S(1)}, bf16[256,1280]{1,0:T(8,128)(2,1)S(1)}, u32[]{:S(2)}, u32[]{:S(2)}) collective-permute-start(bf16[256,1280]{1,0:T(8,128)(2,1)S(1)} %slice.65.refs_2_), channel_id=1, source_target_pairs={{0,2},{1,3},{2,0},{3,1},{4,6},{5,7},{6,4},{7,5},{8,10},{9,11},{10,... | collective-permute-start | bytes 1966088 | tf_op jit(solution)/shard_map/ppermute | solution.py:199
  65.0 37.7 %collective-permute-start.17 = (bf16[2048,256]{1,0:T(8,128)(2,1)}, bf16[2048,256]{1,0:T(8,128)(2,1)}, u32[]{:S(2)}, u32[]{:S(2)}) collective-permute-start(bf16[2048,256]{1,0:T(8,128)(2,1)} %bitcast.32.refs_0_), channel_id=1, source_target_pairs={{0,2},{1,3},{2,0},{3,1},{4,6},{5,7},{6,4},{7,5},{8,10},{9,11},{10,... | collective-permute-start | bytes 3145736 | tf_op jit(solution)/shard_map/ppermute | solution.py:199
  65.5 56.0 %collective-permute-start.19 = (bf16[2048,256]{1,0:T(8,128)(2,1)}, bf16[2048,256]{1,0:T(8,128)(2,1)}, u32[]{:S(2)}, u32[]{:S(2)}) collective-permute-start(bf16[2048,256]{1,0:T(8,128)(2,1)} %bitcast.33.refs_2_), channel_id=1, source_target_pairs={{0,2},{1,3},{2,0},{3,1},{4,6},{5,7},{6,4},{7,5},{8,10},{9,11},{10,... | collective-permute-start | bytes 3145736 | tf_op jit(solution)/shard_map/ppermute | solution.py:199
  67.0 14.0 %collective-permute-start.2 = (bf16[2,2,64,1024]{3,2,1,0:T(8,128)(2,1)S(1)}, bf16[2,2,64,1024]{3,2,1,0:T(8,128)(2,1)S(1)}, u32[]{:S(2)}, u32[]{:S(2)}) collective-permute-start(bf16[2,2,64,1024]{3,2,1,0:T(8,128)(2,1)S(1)} %get-tuple-element.31), channel_id=1, source_target_pairs={{0,8},{4,12},{8,0},{12,4},{16,24},{20,28},{24,16},{28,20},{1,9},{5... | collective-permute-start | bytes 1572872 | tf_op jit(solution)/shard_map/ppermute | solution.py:199
  67.0 14.5 %collective-permute-start.5 = (bf16[2,2,64,1152]{3,2,0,1:T(8,128)(2,1)S(1)}, bf16[2,2,64,1152]{3,2,0,1:T(8,128)(2,1)S(1)}, u32[]{:S(2)}, u32[]{:S(2)}) collective-permute-start(bf16[2,2,64,1152]{3,2,0,1:T(8,128)(2,1)S(1)} %get-tuple-element.29), channel_id=1, source_target_pairs={{0,4},{4,0},{8,12},{12,8},{16,20},{20,16},{24,28},{28,24},{1,5},{5... | collective-permute-start | bytes 1769480 | tf_op jit(solution)/shard_map/ppermute | solution.py:199
  80.1 0.9 copy-start.2
  81.0 42.3 %collective-permute-start.15 = (bf16[2048,256]{1,0:T(8,128)(2,1)}, bf16[2048,256]{1,0:T(8,128)(2,1)}, u32[]{:S(2)}, u32[]{:S(2)}) collective-permute-start(bf16[2048,256]{1,0:T(8,128)(2,1)} %bitcast.32.refs_0_), channel_id=1, source_target_pairs={{0,1},{1,0},{2,3},{3,2},{4,5},{5,4},{6,7},{7,6},{8,9},{9,8},{10,11... | collective-permute-start | bytes 3145736 | tf_op jit(solution)/shard_map/ppermute | solution.py:199
  81.0 0.8 copy-start.18
  81.0 42.9 %collective-permute-start.16 = (bf16[2048,256]{1,0:T(8,128)(2,1)}, bf16[2048,256]{1,0:T(8,128)(2,1)}, u32[]{:S(2)}, u32[]{:S(2)}) collective-permute-start(bf16[2048,256]{1,0:T(8,128)(2,1)} %bitcast.33.refs_2_), channel_id=1, source_target_pairs={{0,1},{1,0},{2,3},{3,2},{4,5},{5,4},{6,7},{7,6},{8,9},{9,8},{10,11... | collective-permute-start | bytes 3145736 | tf_op jit(solution)/shard_map/ppermute | solution.py:199
  81.8 0.8 copy-start.14
  82.7 43.0 %collective-permute-start.13 = (bf16[2,128,2048]{2,1,0:T(8,128)(2,1)}, bf16[2,128,2048]{2,1,0:T(8,128)(2,1)}, u32[]{:S(2)}, u32[]{:S(2)}) collective-permute-start(bf16[2,128,2048]{2,1,0:T(8,128)(2,1)} %dynamic-slice_bitcast_fusion), channel_id=1, source_target_pairs={{0,1},{1,0},{2,3},{3,2},{4,5},{5,4},{6,7},{7,6},{8,9},{9,8},{10,11... | collective-permute-start | bytes 3145736 | tf_op jit(solution)/shard_map/ppermute | solution.py:199
  102.7 33.0 %collective-permute-start.18 = (bf16[2048,256]{1,0:T(8,128)(2,1)}, bf16[2048,256]{1,0:T(8,128)(2,1)S(1)}, u32[]{:S(2)}, u32[]{:S(2)}) collective-permute-start(bf16[2048,256]{1,0:T(8,128)(2,1)} %collective-permute-done.17.refs_0_), channel_id=1, source_target_pairs={{0,1},{1,0},{2,3},{3,2},{4,5},{5,4},{6,7},{7,6},{8,9},{9,8},{10,11... | collective-permute-start | bytes 3145736 | tf_op jit(solution)/shard_map/ppermute | solution.py:199
  121.5 14.6 %collective-permute-start.20 = (bf16[2048,256]{1,0:T(8,128)(2,1)}, bf16[2048,256]{1,0:T(8,128)(2,1)S(1)}, u32[]{:S(2)}, u32[]{:S(2)}) collective-permute-start(bf16[2048,256]{1,0:T(8,128)(2,1)} %collective-permute-done.19.refs_2_), channel_id=1, source_target_pairs={{0,1},{1,0},{2,3},{3,2},{4,5},{5,4},{6,7},{7,6},{8,9},{9,8},{10,11... | collective-permute-start | bytes 3145736 | tf_op jit(solution)/shard_map/ppermute | solution.py:199
  121.5 1.5 copy-start.12
  121.5 1.6 copy-start.15
  123.1 1.0 copy-start.1
  123.1 2.5 %copy-start.3 = (bf16[256,1280]{1,0:T(8,128)(2,1)S(1)}, bf16[256,1280]{1,0:T(8,128)(2,1)}, u32[]{:S(2)}) copy-start(bf16[256,1280]{1,0:T(8,128)(2,1)} %copy-done.2) | copy-start | bytes 1966084
  123.3 17.0 %collective-permute-start.25 = (bf16[256,1280]{1,0:T(8,128)(2,1)S(1)}, bf16[256,1280]{1,0:T(8,128)(2,1)S(1)}, u32[]{:S(2)}, u32[]{:S(2)}) collective-permute-start(bf16[256,1280]{1,0:T(8,128)(2,1)S(1)} %slice.65.refs_2_), channel_id=1, source_target_pairs={{0,1},{1,0},{2,3},{3,2},{4,5},{5,4},{6,7},{7,6},{8,9},{9,8},{10,11... | collective-permute-start | bytes 1966088 | tf_op jit(solution)/shard_map/ppermute | solution.py:199
  124.1 11.5 %collective-permute-start.22 = (bf16[256,768]{1,0:T(8,128)(2,1)S(1)}, bf16[256,768]{1,0:T(8,128)(2,1)S(1)}, u32[]{:S(2)}, u32[]{:S(2)}) collective-permute-start(bf16[256,768]{1,0:T(8,128)(2,1)S(1)} %copy-done.1), channel_id=1, source_target_pairs={{0,2},{1,3},{2,0},{3,1},{4,6},{5,7},{6,4},{7,5},{8,10},{9,11},{10,... | collective-permute-start | bytes 1179656 | tf_op jit(solution)/shard_map/ppermute | solution.py:199
  125.6 14.7 %collective-permute-start.27 = (bf16[256,1280]{1,0:T(8,128)(2,1)S(1)}, bf16[256,1280]{1,0:T(8,128)(2,1)S(1)}, u32[]{:S(2)}, u32[]{:S(2)}) collective-permute-start(bf16[256,1280]{1,0:T(8,128)(2,1)S(1)} %copy-done.3), channel_id=1, source_target_pairs={{0,1},{1,0},{2,3},{3,2},{4,5},{5,4},{6,7},{7,6},{8,9},{9,8},{10,11... | collective-permute-start | bytes 1966088 | tf_op jit(solution)/shard_map/ppermute | solution.py:199
  135.6 7.6 %collective-permute-start.21 = (bf16[256,768]{1,0:T(8,128)(2,1)S(1)}, bf16[256,768]{1,0:T(8,128)(2,1)S(1)}, u32[]{:S(2)}, u32[]{:S(2)}) collective-permute-start(bf16[256,768]{1,0:T(8,128)(2,1)S(1)} %copy-done.1), channel_id=1, source_target_pairs={{0,1},{1,0},{2,3},{3,2},{4,5},{5,4},{6,7},{7,6},{8,9},{9,8},{10,11... | collective-permute-start | bytes 1179656 | tf_op jit(solution)/shard_map/ppermute | solution.py:199
  135.6 7.6 %collective-permute-start.23 = (bf16[256,768]{1,0:T(8,128)(2,1)S(1)}, bf16[256,768]{1,0:T(8,128)(2,1)S(1)}, u32[]{:S(2)}, u32[]{:S(2)}) collective-permute-start(bf16[256,768]{1,0:T(8,128)(2,1)S(1)} %collective-permute-done.22.refs_4_), channel_id=1, source_target_pairs={{0,1},{1,0},{2,3},{3,2},{4,5},{5,4},{6,7},{7,6},{8,9},{9,8},{10,11... | collective-permute-start | bytes 1179656 | tf_op jit(solution)/shard_map/ppermute | solution.py:199
  142.3 18.4 %collective-permute-start.28 = (bf16[2,2,64,1280]{3,2,0,1:T(8,128)(2,1)S(1)}, bf16[2,2,64,1280]{3,2,0,1:T(8,128)(2,1)S(1)}, u32[]{:S(2)}, u32[]{:S(2)}) collective-permute-start(bf16[2,2,64,1280]{3,2,0,1:T(8,128)(2,1)S(1)} %bitcast.138), channel_id=1, source_target_pairs={{0,4},{4,0},{8,12},{12,8},{16,20},{20,16},{24,28},{28,24},{1,5},{5... | collective-permute-start | bytes 1966088 | tf_op jit(solution)/shard_map/ppermute | solution.py:199
  144.4 10.8 %collective-permute-start.31 = (bf16[2,2,64,768]{3,2,1,0:T(8,128)(2,1)S(1)}, bf16[2,2,64,768]{3,2,1,0:T(8,128)(2,1)S(1)}, u32[]{:S(2)}, u32[]{:S(2)}) collective-permute-start(bf16[2,2,64,768]{3,2,1,0:T(8,128)(2,1)S(1)} %slice_bitcast_fusion), channel_id=1, source_target_pairs={{0,8},{4,12},{8,0},{12,4},{16,24},{20,28},{24,16},{28,20},{1,9},{5... | collective-permute-start | bytes 1179656 | tf_op jit(solution)/shard_map/ppermute | solution.py:199
  144.9 14.9 %collective-permute-start.24 = (bf16[128,2048]{1,0:T(8,128)(2,1)S(1)}, bf16[128,2048]{1,0:T(8,128)(2,1)S(1)}, u32[]{:S(2)}, u32[]{:S(2)}) collective-permute-start(bf16[128,2048]{1,0:T(8,128)(2,1)S(1)} %dynamic-slice_bitcast_fusion.1), channel_id=1, source_target_pairs={{0,2},{1,3},{2,0},{3,1},{4,6},{5,7},{6,4},{7,5},{8,10},{9,11},{10,... | collective-permute-start | bytes 1572872 | tf_op jit(solution)/shard_map/ppermute | solution.py:199
  146.5 34.5 %collective-permute-start.34 = (bf16[64,2048]{1,0:T(8,128)(2,1)S(1)}, bf16[64,2048]{1,0:T(8,128)(2,1)S(1)}, u32[]{:S(2)}, u32[]{:S(2)}) collective-permute-start(bf16[64,2048]{1,0:T(8,128)(2,1)S(1)} %dynamic-slice_bitcast_fusion.3), channel_id=1, source_target_pairs={{0,2},{1,3},{2,0},{3,1},{4,6},{5,7},{6,4},{7,5},{8,10},{9,11},{10,... | collective-permute-start | bytes 786440 | tf_op jit(solution)/shard_map/ppermute | solution.py:199
  155.4 10.7 %collective-permute-start.32 = (bf16[2,64,768]{2,1,0:T(8,128)(2,1)S(1)}, bf16[2,64,768]{2,1,0:T(8,128)(2,1)S(1)}, u32[]{:S(2)}, u32[]{:S(2)}) collective-permute-start(bf16[2,64,768]{2,1,0:T(8,128)(2,1)S(1)} %slice_bitcast_fusion.4), channel_id=1, source_target_pairs={{0,16},{4,20},{8,24},{12,28},{16,0},{20,4},{24,8},{28,12},{1,17},{... | collective-permute-start | bytes 589832 | tf_op jit(solution)/shard_map/ppermute | solution.py:199
  160.8 11.3 %collective-permute-start.29 = (bf16[2,64,1280]{2,1,0:T(8,128)(2,1)S(1)}, bf16[2,64,1280]{2,1,0:T(8,128)(2,1)S(1)}, u32[]{:S(2)}, u32[]{:S(2)}) collective-permute-start(bf16[2,64,1280]{2,1,0:T(8,128)(2,1)S(1)} %slice_bitcast_fusion.2), channel_id=1, source_target_pairs={{0,8},{4,12},{8,0},{12,4},{16,24},{20,28},{24,16},{28,20},{1,9},{5... | collective-permute-start | bytes 983048 | tf_op jit(solution)/shard_map/ppermute | solution.py:199
  166.2 6.2 %collective-permute-start.33 = (bf16[64,768]{1,0:T(8,128)(2,1)S(1)}, bf16[64,768]{1,0:T(8,128)(2,1)S(1)}, u32[]{:S(2)}, u32[]{:S(2)}) collective-permute-start(bf16[64,768]{1,0:T(8,128)(2,1)S(1)} %slice_bitcast_fusion.8), channel_id=1, source_target_pairs={{0,4},{4,0},{8,12},{12,8},{16,20},{20,16},{24,28},{28,24},{1,5},{5... | collective-permute-start | bytes 294920 | tf_op jit(solution)/shard_map/ppermute | solution.py:199
  172.2 8.7 %collective-permute-start.30 = (bf16[64,1280]{1,0:T(8,128)(2,1)S(1)}, bf16[64,1280]{1,0:T(8,128)(2,1)S(1)}, u32[]{:S(2)}, u32[]{:S(2)}) collective-permute-start(bf16[64,1280]{1,0:T(8,128)(2,1)S(1)} %slice_bitcast_fusion.6), channel_id=1, source_target_pairs={{0,16},{4,20},{8,24},{12,28},{16,0},{20,4},{24,8},{28,12},{1,17},{... | collective-permute-start | bytes 491528 | tf_op jit(solution)/shard_map/ppermute | solution.py:199
